TPU v7x, 512 devices: a whole 4x4x16 slice. The times are simulated.
512 devices in a mesh: rep: 2 (over z_hi), fs: 32 (over z_lo, y), tp: 8 (over x, core).
Axes of the slice: x: 4, y: 4, z: 16 (z_hi: 2, z_lo: 8; z = z_hi * 8 + z_lo), core: 2. Of those that a mesh axis runs over, the one named last changes fastest.
Arguments:
- tokens: bfloat16 [32768, 2048], P(('rep', 'fs')), may hold values from -6 to 6
- gate_outer: bfloat16 [2048, 1024], P('fs', 'tp'), may hold values from -0.125 to 0.125
- gate_inner: bfloat16 [2048, 1024], P('fs', 'tp'), may hold values from -0.125 to 0.125
- conv_input: bfloat16 [2048, 1024], P('fs', 'tp'), may hold values from -0.125 to 0.125
- mixer_output: bfloat16 [2048, 1024], P('fs', 'tp'), may hold values from -0.1875 to 0.1875
- conv_taps: float32 [3, 1024], P(None, 'tp'), may hold values from -3 to 3
- mixer_gain: float32 [2048], replicated, may hold values from 0.1 to 1.9
- mixer_shift: float32 [2048], replicated, may hold values from -3 to 3
- up_weight: bfloat16 [2048, 8192], P('fs', 'tp'), may hold values from -0.125 to 0.125
- down_weight: bfloat16 [2048, 8192], P('fs', 'tp'), may hold values from -0.0625 to 0.0625
- channel_gain: float32 [2048], replicated, may hold values from 0.1 to 1.9
- channel_shift: float32 [2048], replicated, may hold values from -3 to 3
Outputs:
- mixed: bfloat16 [32768, 2048], P(('rep', 'fs'))
All inputs are finite; a program needn't handle non-finite values.
Results may differ from a plain program's by a relative error of at most 0.014.
Values may be sent and summed in bfloat16 or wider, within the bound.
A program may use at most 64 MiB of HBM per device.

v0:
```python
import jax
import jax.numpy as jnp
from jax import lax
from jax.sharding import PartitionSpec as P

residual_scale = 8.0**0.25
norm_epsilon = 1e-05


def in_one_piece(arrays, axis, dim, along):
    ends, at = ([], 0)
    for a in arrays[:-1]:
        at += a.shape[along]
        ends.append(at)
    both = jnp.concatenate(arrays, axis=along)
    return tuple(jnp.split(lax.all_gather(both, axis, axis=dim, tiled=True), ends, axis=along))


def cut_along(array, dim, count):
    before, after = (array.shape[:dim], array.shape[dim + 1 :])
    return jnp.moveaxis(array.reshape(*before, count, -1, *after), dim, 0)


def sum_at_owner(array, axis, dim):
    count = lax.axis_size(axis)
    tiles = lax.all_to_all(cut_along(array, dim, count), axis, 0, 0, tiled=True)
    return jnp.sum(tiles.astype(jnp.float32), axis=0)


def from_everyone(array, axis):
    copies = jnp.broadcast_to(array, (lax.axis_size(axis), *array.shape))
    return lax.all_to_all(copies, axis, split_axis=0, concat_axis=0, tiled=True)


def laid_out(tiles, dim):
    shape = list(tiles.shape[1:])
    shape[dim] *= tiles.shape[0]
    return jnp.moveaxis(tiles, 0, dim).reshape(shape)


def collect(array, axis, dim):
    tiles = from_everyone(array, axis)
    return laid_out(tiles, dim)


def layer_norm(values, gain, shift):
    row_mean = jnp.mean(values, -1, keepdims=True)
    centered = values - row_mean
    variance = jnp.mean(centered * centered, -1, keepdims=True)
    return centered * lax.rsqrt(variance + norm_epsilon) * gain + shift


def rounded_partial(left, right_t):
    product = lax.dot_general(
        left, right_t, (((1,), (1,)), ((), ())), preferred_element_type=jnp.float32
    )
    return lax.optimization_barrier(product.astype(jnp.bfloat16)).astype(jnp.float32)


def gated_conv(outer_gate, inner_gate, conv_values, conv_taps):
    seq_len = conv_values.shape[0]
    tap_count = conv_taps.shape[0]
    product = inner_gate * conv_values
    padded = jnp.pad(product, ((tap_count - 1, 0), (0, 0)))
    result = jnp.zeros_like(product)
    for tap_index in range(tap_count):
        result = result + conv_taps[tap_index] * padded[tap_index : tap_index + seq_len]
    return (outer_gate * result).astype(jnp.bfloat16)


def local(
    tokens,
    gate_outer,
    gate_inner,
    conv_input,
    mixer_output,
    conv_taps,
    mixer_gain,
    mixer_shift,
    up_weight,
    down_weight,
    channel_gain,
    channel_shift,
):
    seq_len = tokens.shape[0]
    own_rows = seq_len // lax.axis_size("tp")
    own_start = lax.axis_index("tp") * own_rows
    own_tokens = lax.dynamic_slice_in_dim(tokens, own_start, own_rows, 0)
    weights_all = in_one_piece(
        (gate_outer, gate_inner, conv_input, mixer_output, up_weight, down_weight), "fs", 0, 1
    )
    outer_gate = jnp.dot(tokens, weights_all[0], preferred_element_type=jnp.float32)
    inner_gate = jnp.dot(tokens, weights_all[1], preferred_element_type=jnp.float32)
    conv_values = jnp.dot(tokens, weights_all[2], preferred_element_type=jnp.float32)
    output_weight = weights_all[3]
    up_full = weights_all[4]
    down_full = weights_all[5]
    conv_out = gated_conv(outer_gate, inner_gate, conv_values, conv_taps)
    mixer_sum = sum_at_owner(rounded_partial(conv_out, output_weight).astype(jnp.bfloat16), "tp", 0)
    first_own = layer_norm(
        residual_scale * own_tokens.astype(jnp.float32) + mixer_sum, mixer_gain, mixer_shift
    ).astype(jnp.bfloat16)
    first_rows = collect(first_own, "tp", 0)
    up_product = jnp.dot(first_rows, up_full, preferred_element_type=jnp.float32)
    hidden = jnp.square(jax.nn.relu(up_product)).astype(jnp.bfloat16)
    channel_sum = sum_at_owner(rounded_partial(hidden, down_full).astype(jnp.bfloat16), "tp", 0)
    output_own = layer_norm(
        residual_scale * first_own.astype(jnp.float32) + channel_sum, channel_gain, channel_shift
    ).astype(jnp.bfloat16)
    return collect(output_own, "tp", 0)


def solution(mesh):
    in_specs = (
        P(("rep", "fs"), None),
        P("fs", "tp"),
        P("fs", "tp"),
        P("fs", "tp"),
        P("fs", "tp"),
        P(None, "tp"),
        P(),
        P(),
        P("fs", "tp"),
        P("fs", "tp"),
        P(),
        P(),
    )
    out_specs = P(("rep", "fs"), None)
    return jax.shard_map(local, mesh=mesh, in_specs=in_specs, out_specs=out_specs, check_vma=False)
```

profile of v0, /device:TPU:1, one launch (start us, length us, event | category | flops | bytes accessed | tf_op | source)
XLA Modules:
  0.0 408.5 jit_solution(9750319974317531724)
XLA Ops:
  6.5 0.9 constant_dynamic-update-slice_fusion.5
  7.4 0.7 constant_dynamic-update-slice_fusion.4
  8.1 0.7 constant_dynamic-update-slice_fusion.3
  8.9 0.7 constant_dynamic-update-slice_fusion.2
  9.6 0.9 constant_dynamic-update-slice_fusion.1
  10.5 0.9 constant_dynamic-update-slice_fusion
  11.4 0.7 copy-done.1
  12.2 0.8 slice_bitcast_fusion.2
  13.0 224.7 %all-gather.2.cloned.1.call-done = bf16[2048,2560]{1,0:T(8,128)(2,1)} async-done(((bf16[64,2560]{1,0:T(8,128)(2,1)}), bf16[2048,2560]{1,0:T(8,128)(2,1)}) %all-gather.2.cloned.1.call-update) | async-done | bytes 10485776 | tf_op jit(solution)/shard_map/all_gather | solution.py:16
  237.7 2.6 fusion.17
  240.3 1.9 fusion.11
  242.2 4.0 convolution_convert_fusion
  246.2 24.4 %all-to-all-start = ((bf16[8,64,2048]{2,1,0:T(8,128)(2,1)}), bf16[8,64,2048]{2,1,0:T(8,128)(2,1)}, u32[]{:S(2)}, u32[]{:S(2)}) async-start(bf16[8,64,2048]{2,1,0:T(8,128)(2,1)} %bitcast.24), calls=%async_computation | async-start | bytes 4194304 | tf_op jit(solution)/shard_map/all_to_all | solution.py:26
  270.6 26.3 %all-to-all-done = bf16[8,64,2048]{2,1,0:T(8,128)(2,1)} async-done(((bf16[8,64,2048]{2,1,0:T(8,128)(2,1)}), bf16[8,64,2048]{2,1,0:T(8,128)(2,1)}, u32[]{:S(2)}, u32[]{:S(2)}) %all-to-all-start) | async-done | bytes 2097184 | tf_op jit(solution)/shard_map/all_to_all | solution.py:26
  296.9 2.0 convert_reduce_fusion.1
  299.6 0.2 broadcast_in_dim.4
  299.8 29.6 %all_to_all.20 = bf16[8,64,2048]{2,1,0:T(8,128)(2,1)S(1)} all-to-all(bf16[8,64,2048]{2,1,0:T(8,128)(2,1)S(1)} %broadcast_in_dim.4), channel_id=1, replica_groups=mesh['rep'=2,'fs'=32,'tp'=8] {'tp'}, dimensions={0} | all-to-all | bytes 4194304 | tf_op jit(solution)/shard_map/all_to_all | solution.py:32
  329.4 9.3 %fusion.4 = bf16[512,2048]{1,0:T(8,128)(2,1)} fusion(bf16[2048,2560]{1,0:T(8,128)(2,1)} %all-gather.2.cloned.1.call-done, bf16[512,2048]{1,0:T(8,128)(2,1)S(1)} %bitcast.26), kind=kOutput, calls=%fused_computation.6 | convolution fusion | flops 4297588736 | bytes 12582912 | tf_op jit(solution)/shard_map/dot_general | solution.py:54
  338.7 30.7 %all_to_all.21 = bf16[8,64,2048]{2,1,0:T(8,128)(2,1)S(1)} all-to-all(bf16[8,64,2048]{2,1,0:T(8,128)(2,1)} %bitcast.27), channel_id=1, replica_groups=mesh['rep'=2,'fs'=32,'tp'=8] {'tp'}, dimensions={0} | all-to-all | bytes 4194304 | tf_op jit(solution)/shard_map/all_to_all | solution.py:26
  369.4 0.4 convert_reduce_fusion
  370.0 0.2 multiply_reduce_fusion
  370.4 0.2 broadcast_in_dim.5
  370.6 29.7 %all_to_all.22 = bf16[8,64,2048]{2,1,0:T(8,128)(2,1)S(1)} all-to-all(bf16[8,64,2048]{2,1,0:T(8,128)(2,1)S(1)} %broadcast_in_dim.5), channel_id=1, replica_groups=mesh['rep'=2,'fs'=32,'tp'=8] {'tp'}, dimensions={0} | all-to-all | bytes 4194304 | tf_op jit(solution)/shard_map/all_to_all | solution.py:32
  400.3 1.3 copy.19
  (22 shorter events, 1.0 us)
Async XLA Ops:
  6.5 233.7 %copy-start = (bf16[512,2048]{1,0:T(8,128)(2,1)S(1)}, bf16[512,2048]{1,0:T(8,128)(2,1)}, u32[]{:S(2)}) copy-start(bf16[512,2048]{1,0:T(8,128)(2,1)} %param.12) | copy-start | bytes 6291460
  6.5 231.1 %all-gather.2.cloned.1.call-start = ((), (), s32[]{:S(2)}) async-start(), calls=%async_computation.4 | async-start | bytes 10813440 | tf_op jit(solution)/shard_map/all_gather | solution.py:16
  11.4 0.7 copy-start.1
  246.2 50.7 %all-to-all-start = ((bf16[8,64,2048]{2,1,0:T(8,128)(2,1)}), bf16[8,64,2048]{2,1,0:T(8,128)(2,1)}, u32[]{:S(2)}, u32[]{:S(2)}) async-start(bf16[8,64,2048]{2,1,0:T(8,128)(2,1)} %bitcast.24), calls=%async_computation | async-start | bytes 4194304 | tf_op jit(solution)/shard_map/all_to_all | solution.py:26
  270.6 28.8 %copy-start.2 = (f32[2048]{0:T(1024)S(1)}, f32[2048]{0:T(1024)}, u32[]{:S(2)}) copy-start(f32[2048]{0:T(1024)} %param.19) | copy-start | bytes 24580
  270.6 28.8 %copy-start.3 = (f32[2048]{0:T(1024)S(1)}, f32[2048]{0:T(1024)}, u32[]{:S(2)}) copy-start(f32[2048]{0:T(1024)} %param.18) | copy-start | bytes 24580
  369.4 0.8 copy-start.4
  369.4 0.8 copy-start.5
Sparse Core Ops, SparseCore 0:
  12.3 225.3 all-gather.1
where the time goes:
time: 409 us; the launch traced here: 408 us
  waiting for transfers between devices  251 us (61%)
  blocking collectives  89.9 us (22%)
  starting transfers between devices  24.4 us (6%)
  matrix products  17.8 us (4%)
  between operations  13.5 us (3%)
  local copies, waits for them, and re-layouts  8.22 us (2%)
    all_gather x1, waiting for transfers between devices, in_one_piece(): lax.all_gather(both, axis, axis=dim, tiled=True)  225 us
    all_to_all x2, blocking collectives, from_everyone(): return lax.all_to_all(copies, axis, split_axis=0, concat_axis=0, tiled=True)  59.2 us
    all_to_all x1, blocking collectives, sum_at_owner(): tiles = lax.all_to_all(cut_along(array, dim, count), axis, 0, 0, tiled=True)  30.7 us
    all_to_all x1, waiting for transfers between devices, sum_at_owner(): tiles = lax.all_to_all(cut_along(array, dim, count), axis, 0, 0, tiled=True)  26.3 us
    all_to_all x1, starting transfers between devices, sum_at_owner(): tiles = lax.all_to_all(cut_along(array, dim, count), axis, 0, 0, tiled=True)  24.4 us
    dot_general x2, matrix products, rounded_partial(): lax.dot_general(left, right_t, (((1,), (1,)), ((), ())), preferred_elemen...  13.3 us
  transfers between devices with their start and end apart: 2, of which 2 were waited for; matrix products, arithmetic and copies ran while one was open for 0% of the time, Pallas kernels for 0%

commit v1 on v0

v1 whole, which is shorter than its diff:
```python
import functools

import jax
import jax.numpy as jnp
from jax import lax
from jax.experimental import pallas as pl
from jax.experimental.pallas import tpu as pltpu
from jax.sharding import PartitionSpec as P

residual_scale = 8.0**0.25
norm_epsilon = 1e-05

NZ, NY, NX = 8, 4, 4
SEQ, WIDTH = 512, 2048
ROWS = 64
GROUP = 256
CHUNKS, CHUNK = 8, 256
ARRIVAL = (0, 1, -1, 2, -2, 3, -3, 4)

LINK_RATE, LINK_LAT = 46.6e3, 1.9
PAIR_RATE, PAIR_LAT = 500e3, 1.1
BACKLOG = 1.0


class Op:
    def __init__(self, name, deps, emit, prio, dur=0.0, link=None, nbytes=0, wait=None, latency=0.0):
        self.name, self.deps, self.emit, self.prio = name, deps, emit, prio
        self.dur, self.link, self.nbytes, self.wait = dur, link, nbytes, wait
        self.latency = latency


def plan(ops):
    done, link_free, order, now = {}, {}, [], 0.0
    left = list(ops)
    while left:
        best = None
        for at, op in enumerate(left):
            if any(d not in done for d in op.deps):
                continue
            ready = max([done[d] for d in op.deps], default=0.0)
            if op.link is not None:
                ready = max(ready, link_free.get(op.link, 0.0) - BACKLOG)
            key = (max(ready, now), op.prio, at)
            if best is None or key < best[0]:
                best = (key, op)
        (start, _, _), op = best
        left.remove(op)
        now = start + (op.dur if op.link is None else 0.02)
        if op.link is None:
            done[op.name] = now + op.latency
        else:
            rate, lat = (PAIR_RATE, PAIR_LAT) if op.link == "c" else (LINK_RATE, LINK_LAT)
            begin = max(now, link_free.get(op.link, 0.0))
            link_free[op.link] = begin + op.nbytes / rate
            done[op.name] = link_free[op.link] + lat
        order.append((start, op))
    return order, done


def layer_kernel(
    tok_hbm, go_hbm, gi_hbm, ci_hbm, mo_hbm, up_hbm, dn_hbm, taps, mgain, mshift, cgain, cshift,
    out_hbm,
    tok, wm, wu, wd, proj, prod, conv, ps, so, dr, rl, fr, fd, v, first, hid, res,
    send_sems, recv_sems, load_sems, store_sems,
    report=None,
):
    f32, bf16 = jnp.float32, jnp.bfloat16
    rep, fs, tp = lax.axis_index("rep"), lax.axis_index("fs"), lax.axis_index("tp")
    zl, y = lax.div(fs, NY), lax.rem(fs, NY)
    x, c = lax.div(tp, 2), lax.rem(tp, 2)
    z = rep * NZ + zl

    def mod(v, n):
        return lax.rem(v + 2 * n, n)

    def device(dz=0, dy=0, dx=0, dc=0):
        zz = mod(z + dz, 2 * NZ)
        return (
            lax.div(zz, NZ),
            lax.rem(zz, NZ) * NY + mod(y + dy, NY),
            mod(x + dx, NX) * 2 + lax.rem(c + dc, 2),
        )

    peer = {
        "z+": device(dz=1), "z-": device(dz=-1), "y+": device(dy=1), "y-": device(dy=-1),
        "x+": device(dx=1), "x-": device(dx=-1), "c": device(dc=1),
    }
    sign = {"+": 1, "-": -1}

    ops = []
    sends = []

    def send(name, link, deps, src, dst, landed, nbytes, prio):
        index = len(sends)

        def copy(s, d):
            return pltpu.make_async_remote_copy(
                src_ref=s, dst_ref=d, send_sem=send_sems.at[index], recv_sem=recv_sems.at[index],
                device_id=peer[link], device_id_type=pl.DeviceIdType.MESH,
            )

        sends.append((name, lambda: copy(src(), dst()).wait_send()))
        ops.append(Op(
            name, deps, lambda: copy(src(), dst()).start(), prio, link=link, nbytes=nbytes,
            wait=lambda: copy(landed(), landed()).wait_recv(),
        ))

    def compute(name, deps, emit, prio, dur):
        ops.append(Op(name, deps, emit, prio, dur=dur))

    loads = []

    def load(name, src, dst):
        index = len(loads)
        op = Op(name, [], lambda: None, 0, latency=0.5)
        op.wait = lambda: pltpu.make_async_copy(src(), dst(), load_sems.at[index]).wait()
        loads.append(lambda: pltpu.make_async_copy(src(), dst(), load_sems.at[index]).start())
        ops.append(op)

    def own(w, c0, n):
        return lambda: w.at[zl, pl.ds(pl.multiple_of(y * ROWS, ROWS), ROWS), pl.ds(c0, n)]

    load("load.m0", lambda: go_hbm, own(wm, 0, 128))
    load("load.m1", lambda: gi_hbm, own(wm, 128, 128))
    load("load.m2", lambda: ci_hbm, own(wm, 256, 128))
    load("load.m3", lambda: mo_hbm, own(wm, 384, 128))
    load("load.u", lambda: up_hbm, own(wu, 0, 1024))
    load("load.d", lambda: dn_hbm, own(wd, 0, 1024))
    load("load.t", lambda: tok_hbm, lambda: tok)

    def block(w, dz, dy, c0, n, half=None):
        rows, off = (ROWS, 0) if half is None else (ROWS // 2, half * ROWS // 2)

        def view():
            start = pl.multiple_of(mod(y + dy, NY) * ROWS + off, ROWS // 2)
            return w.at[mod(zl + dz, NZ), pl.ds(start, rows), pl.ds(c0, n)]

        return view

    def slab(w, dz, c0, n, half=None):
        rows, off = (GROUP, 0) if half is None else (GROUP // 2, half * GROUP // 2)
        return lambda: w.at[mod(zl + dz, NZ), pl.ds(off, rows), pl.ds(c0, n)]

    ready = {}

    def y_first(tag, w, c0, n, deps, prio):
        size = ROWS * n * 2
        for d in "+-":
            s = sign[d]
            b = block(w, 0, 0, c0, n)
            send(f"{tag}.Y1{d}", "y" + d, deps, b, b, block(w, 0, -s, c0, n), size, prio)
        for d, half in (("+", 0), ("-", 1)):
            s = sign[d]
            b = block(w, 0, -s, c0, n, half)
            send(f"{tag}.Y2{d}", "y" + d, [f"{tag}.Y1{d}"], b, b, block(w, 0, -2 * s, c0, n, half), size // 2, prio)
        group = [f"{tag}.Y{h}{d}" for h in (1, 2) for d in "+-"]
        ready[tag[0], 0] = ready.get((tag[0], 0), []) + group
        for d, half in (("+", 0), ("-", 1)):
            s = sign[d]
            for h in (1, 2, 3, 4):
                part = half if h == 4 else None
                b = slab(w, -s * (h - 1), c0, n, part)
                before = deps + group if h == 1 else [f"{tag}.Z{h - 1}{d}"]
                send(f"{tag}.Z{h}{d}", "z" + d, before, b, b, slab(w, -s * h, c0, n, part),
                     NY * size // (1 if part is None else 2), prio)
                dist = 4 if h == 4 else -s * h
                ready[tag[0], dist] = ready.get((tag[0], dist), []) + [f"{tag}.Z{h}{d}"]

    def z_first(tag, w, c0, n, deps, prio):
        size = ROWS * n * 2
        for d, half in (("+", 0), ("-", 1)):
            s = sign[d]
            for h in (1, 2, 3, 4):
                part = half if h == 4 else None
                b = block(w, -s * (h - 1), 0, c0, n, part)
                before = deps if h == 1 else [f"{tag}.Z{h - 1}{d}"]
                send(f"{tag}.Z{h}{d}", "z" + d, before, b, b, block(w, -s * h, 0, c0, n, part),
                     size // (1 if part is None else 2), prio)
        for dist in ARRIVAL:
            here = {0: deps, 4: [f"{tag}.Z4+", f"{tag}.Z4-"]}.get(
                dist, [f"{tag}.Z{abs(dist)}{'-' if dist > 0 else '+'}"])
            for d, half in (("+", 0), ("-", 1)):
                s = sign[d]
                b = block(w, dist, 0, c0, n)
                send(f"{tag}.Y1{d}{dist}", "y" + d, here, b, b, block(w, dist, -s, c0, n), size, prio)
                b = block(w, dist, -s, c0, n, half)
                send(f"{tag}.Y2{d}{dist}", "y" + d, [f"{tag}.Y1{d}{dist}"], b, b,
                     block(w, dist, -2 * s, c0, n, half), size // 2, prio)
            names = here + [f"{tag}.Y{h}{d}{dist}" for h in (1, 2) for d in "+-"]
            ready[tag[0], dist] = ready.get((tag[0], dist), []) + names

    mixer_loads = ["load.m0", "load.m1", "load.m2", "load.m3"]
    y_first("my", wm, 0, 256, ["load.m0", "load.m1"], 1)
    z_first("mz", wm, 256, 256, ["load.m2", "load.m3"], 1)
    y_first("uy", wu, 0, 384, ["load.u"], 3)
    z_first("uz", wu, 384, 640, ["load.u"], 3)
    y_first("dy", wd, 0, 384, ["load.d"], 5)
    z_first("dz", wd, 384, 640, ["load.d"], 5)

    def project():
        def step(i, _):
            rows = pl.ds(pl.multiple_of(i * 128, 128), 128)
            proj[rows, :] = jnp.dot(
                tok[rows, :], wm[:, :, 0:384].reshape(WIDTH, 384), preferred_element_type=f32)
            return 0

        lax.fori_loop(0, SEQ // 128, step, 0)
        prod[0:8, :] = jnp.zeros((8, 128), f32)
        prod[8:, :] = proj[:, 128:256] * proj[:, 256:384]
        total = taps[0:1, :] * prod[6:6 + SEQ, :]
        total = total + taps[1:2, :] * prod[7:7 + SEQ, :]
        total = total + taps[2:3, :] * prod[8:8 + SEQ, :]
        conv[...] = (proj[:, 0:128] * total).astype(bf16)

    mixer_ready = [n for dist in ARRIVAL for n in ready["m", dist]]
    compute("project", ["load.t"] + mixer_loads + mixer_ready, project, 0, 3.0)

    half_rows = lambda which: pl.ds(pl.multiple_of(which * GROUP, GROUP), GROUP)
    nt = (((1,), (1,)), ((), ()))

    def product(phase, k, left, right):
        weight = right()
        ps[phase, k] = lax.dot_general(
            left[half_rows(1 - c), :], weight, nt, preferred_element_type=f32).astype(bf16)
        so[phase, k] = lax.dot_general(
            left[half_rows(c), :], weight, nt, preferred_element_type=f32).astype(bf16)

    def rows_of(dx):
        return pl.ds(pl.multiple_of(mod(x + dx, NX) * ROWS, ROWS), ROWS)

    def own_rows():
        return pl.ds(pl.multiple_of((c * NX + x) * ROWS, ROWS), ROWS)

    def sum_chunk(phase, k, column, residual, prio):
        t = f"s{phase}.{k}"
        d, e = ("+", "-") if k % 2 == 0 else ("-", "+")
        s = sign[d]
        send(f"{t}.pair", "c", [f"{t}.product"], lambda: ps.at[phase, k], lambda: dr.at[phase, k],
             lambda: dr.at[phase, k], GROUP * CHUNK * 2, prio)

        def add_pair():
            so[phase, k] = (so[phase, k].astype(f32) + dr[phase, k].astype(f32)).astype(bf16)

        compute(f"{t}.add", [f"{t}.product", f"{t}.pair"], add_pair, prio, 0.15)
        size = ROWS * CHUNK * 2
        at = lambda dx: (lambda: so.at[phase, k, rows_of(dx), :])
        slot = lambda ref: (lambda: ref.at[phase, k])
        send(f"{t}.relay", "x" + d, [f"{t}.add"], at(2), slot(rl), slot(rl), size, prio)
        send(f"{t}.direct", "x" + e, [f"{t}.add"], at(-s), slot(fd), slot(fd), size, prio)

        def add_relay():
            so[phase, k, rows_of(s), :] = (
                so[phase, k, rows_of(s), :].astype(f32) + rl[phase, k].astype(f32)).astype(bf16)

        compute(f"{t}.radd", [f"{t}.add", f"{t}.relay"], add_relay, prio, 0.05)
        send(f"{t}.final", "x" + d, [f"{t}.radd"], at(s), slot(fr), slot(fr), size, prio)

        def finish():
            columns = pl.ds(pl.multiple_of(column() * CHUNK, CHUNK), CHUNK)
            total = so[phase, k, rows_of(0), :].astype(f32) + fr[phase, k].astype(f32)
            total = total + fd[phase, k].astype(f32)
            v[:, columns] = residual_scale * residual[own_rows(), columns].astype(f32) + total

        compute(f"{t}.finish", [f"{t}.add", f"{t}.final", f"{t}.direct"], finish, prio, 0.05)

    def norm(phase, gain, shift, dest):
        def emit():
            values = v[...]
            mean = jnp.mean(values, -1, keepdims=True)
            centered = values - mean
            variance = jnp.mean(centered * centered, -1, keepdims=True)
            scaled = centered * lax.rsqrt(variance + norm_epsilon)
            dest[own_rows(), :] = (scaled * gain[...] + shift[...]).astype(bf16)

        compute(f"norm{phase}", [f"s{phase}.{k}.finish" for k in range(CHUNKS)], emit, 0, 0.7)

    HALF = WIDTH // 2

    def gather(phase, ref):
        def at(dx, h, other=False):
            def view():
                core = 1 - c if other else c
                rows = pl.ds(pl.multiple_of((core * NX + mod(x + dx, NX)) * ROWS, ROWS), ROWS)
                return ref.at[rows, :] if h is None else ref.at[rows, pl.ds(h * HALF, HALF)]
            return view

        t, size, landed = f"g{phase}", ROWS * HALF * 2, []
        start = [f"norm{phase}"]
        for d, first_half in (("+", 0), ("-", 1)):
            for h in (first_half, 1 - first_half):
                send(f"{t}.A{d}{h}", "x" + d, start, at(0, h), at(0, h), at(-sign[d], h), size, 0)
                landed.append((f"{t}.A{d}{h}", at(-sign[d], h)))
        send(f"{t}.P", "c", start, at(0, None), at(0, None), at(0, None, True), 2 * size, 0)
        landed.append((f"{t}.P", at(0, None, True)))
        for d, h in (("+", 0), ("-", 1)):
            b = at(-sign[d], h)
            send(f"{t}.B{d}", "x" + d, [f"{t}.A{d}{h}"], b, b, at(2, h), size, 0)
            landed.append((f"{t}.B{d}", at(2, h)))
        for name, dx, h in ((f"{t}.A+0", -1, 0), (f"{t}.A-1", 1, 1), (f"{t}.A+1", -1, 1),
                            (f"{t}.A-0", 1, 0), (f"{t}.B+", 2, 0), (f"{t}.B-", 2, 1)):
            send(f"{name}.P", "c", [name], at(dx, h), at(dx, h), at(dx, h, True), size, 0)
            landed.append((f"{name}.P", at(dx, h, True)))
        return landed, at(0, None)

    for k in range(CHUNKS):
        compute(f"s0.{k}.product", ["project"],
                functools.partial(product, 0, k, conv, lambda k=k: wm[k, :, 384:512]), 1, 0.25)
        sum_chunk(0, k, lambda k=k: k, tok, 0)
    norm(0, mgain, mshift, first)
    landed0, _ = gather(0, first)

    def hidden(n):
        columns = pl.ds(n * 256, 256)
        for r in range(2):
            rows = pl.ds(r * 256, 256)
            up = jnp.dot(first[rows, :], wu[:, :, columns].reshape(WIDTH, 256), preferred_element_type=f32)
            hid[rows, columns] = jnp.square(jnp.maximum(up, 0.0)).astype(bf16)

    up_ready = ["load.u"] + [n for dist in ARRIVAL for n in ready["u", dist]]
    for n in range(4):
        compute(f"hidden{n}", ["norm0"] + [name for name, _ in landed0] + up_ready,
                functools.partial(hidden, n), 2, 1.0)
    for k, dist in enumerate(ARRIVAL):
        group = lambda dist=dist: mod(zl + dist, NZ)
        compute(f"s1.{k}.product", [f"hidden{n}" for n in range(4)] + ["load.d"] + ready["d", dist],
                functools.partial(product, 1, k, hid, lambda group=group: wd[group()]), 1, 0.6)
        sum_chunk(1, k, group, first, 0)
    norm(1, cgain, cshift, res)
    landed1, mine = gather(1, res)

    stores = []

    def store(name, deps, view):
        index = len(stores)

        def copy():
            source = view()
            return pltpu.make_async_copy(source, out_view(view), store_sems.at[index])

        stores.append(copy)
        ops.append(Op(name, deps, lambda: copy().start(), 2, dur=0.02))

    def out_view(view):
        return view(out_hbm)

    def place(dx, h, other):
        def view(ref=res):
            core = 1 - c if other else c
            rows = pl.ds(pl.multiple_of((core * NX + mod(x + dx, NX)) * ROWS, ROWS), ROWS)
            return ref.at[rows, :] if h is None else ref.at[rows, pl.ds(h * HALF, HALF)]
        return view

    store("out.own", ["norm1"], place(0, None, False))
    store("out.P", ["g1.P"], place(0, None, True))
    for name, dx, h in (("g1.A+0", -1, 0), ("g1.A-1", 1, 1), ("g1.A+1", -1, 1),
                        ("g1.A-0", 1, 0), ("g1.B+", 2, 0), ("g1.B-", 2, 1)):
        store(f"out.{name}", [name], place(dx, h, False))
        store(f"out.{name}.P", [f"{name}.P"], place(dx, h, True))

    order, done = plan(ops)
    if report is not None:
        report(order, done, len(sends), len(loads), len(stores))

    for start_load in loads:
        start_load()
    barrier = pltpu.get_barrier_semaphore()
    for link in peer:
        pl.semaphore_signal(barrier, inc=1, device_id=peer[link], device_id_type=pl.DeviceIdType.MESH)
    pl.semaphore_wait(barrier, len(peer))

    by_name = {op.name: op for op in ops}
    waited = set()

    def need(name):
        op = by_name[name]
        if op.wait is not None and name not in waited:
            waited.add(name)
            op.wait()

    for _, op in order:
        for name in op.deps:
            need(name)
        op.emit()
    for op in ops:
        need(op.name)
    for _, wait in sends:
        wait()
    for copy in stores:
        copy().wait()


N_SENDS, N_LOADS, N_STORES = 256, 7, 14


def count_ops():
    return N_SENDS, N_LOADS, N_STORES


def local(tokens, gate_outer, gate_inner, conv_input, mixer_output, conv_taps, mixer_gain,
          mixer_shift, up_weight, down_weight, channel_gain, channel_shift):
    bf16, f32 = jnp.bfloat16, jnp.float32
    vmem, hbm = pl.BlockSpec(memory_space=pltpu.VMEM), pl.BlockSpec(memory_space=pl.ANY)
    return pl.pallas_call(
        layer_kernel,
        out_shape=jax.ShapeDtypeStruct((SEQ, WIDTH), bf16),
        in_specs=[hbm] * 7 + [vmem] * 5,
        out_specs=hbm,
        scratch_shapes=[
            pltpu.VMEM((SEQ, WIDTH), bf16),
            pltpu.VMEM((NZ, GROUP, 512), bf16),
            pltpu.VMEM((NZ, GROUP, 1024), bf16),
            pltpu.VMEM((NZ, GROUP, 1024), bf16),
            pltpu.VMEM((SEQ, 384), f32),
            pltpu.VMEM((SEQ + 8, 128), f32),
            pltpu.VMEM((SEQ, 128), bf16),
            pltpu.VMEM((2, CHUNKS, GROUP, CHUNK), bf16),
            pltpu.VMEM((2, CHUNKS, GROUP, CHUNK), bf16),
            pltpu.VMEM((2, CHUNKS, GROUP, CHUNK), bf16),
            pltpu.VMEM((2, CHUNKS, ROWS, CHUNK), bf16),
            pltpu.VMEM((2, CHUNKS, ROWS, CHUNK), bf16),
            pltpu.VMEM((2, CHUNKS, ROWS, CHUNK), bf16),
            pltpu.VMEM((ROWS, WIDTH), f32),
            pltpu.VMEM((SEQ, WIDTH), bf16),
            pltpu.VMEM((SEQ, 1024), bf16),
            pltpu.VMEM((SEQ, WIDTH), bf16),
            pltpu.SemaphoreType.DMA((N_SENDS,)),
            pltpu.SemaphoreType.DMA((N_SENDS,)),
            pltpu.SemaphoreType.DMA((N_LOADS,)),
            pltpu.SemaphoreType.DMA((N_STORES,)),
        ],
        compiler_params=pltpu.CompilerParams(
            collective_id=0, has_side_effects=True, vmem_limit_bytes=60 * 2**20),
    )(tokens, gate_outer, gate_inner, conv_input, mixer_output, up_weight, down_weight, conv_taps,
      mixer_gain.reshape(1, -1), mixer_shift.reshape(1, -1), channel_gain.reshape(1, -1),
      channel_shift.reshape(1, -1))


def solution(mesh):
    weights = P("fs", "tp")
    in_specs = (
        P(("rep", "fs"), None), weights, weights, weights, weights, P(None, "tp"), P(), P(),
        weights, weights, P(), P(),
    )
    out_specs = P(("rep", "fs"), None)
    return jax.shard_map(local, mesh=mesh, in_specs=in_specs, out_specs=out_specs, check_vma=False)
```

time: 409 us -> 118 us (0.29)
  waiting for transfers between devices: 251 us -> 0 us
  Pallas kernels: 0 us -> 114 us
  blocking collectives: 89.9 us -> 0 us
  starting transfers between devices: 24.4 us -> 0 us
  matrix products: 17.8 us -> 0 us
  between operations: 13.5 us -> 0.01 us
  local copies, waits for them, and re-layouts: 8.22 us -> 3.16 us
    all_gather x1 -> x0, waiting for transfers between devices: 225 us -> none  [in_one_piece(): lax.all_gather(both, axis, axis=dim, tiled=True)]
    pallas_call x0 -> x1, Pallas kernels: none -> 114 us  [local(): pl.pallas_call(layer_kernel, out_shape=jax.ShapeDtypeStruct((SEQ, WIDTH),...]
    all_to_all x3 -> x0, blocking collectives: 89.9 us -> none  [the longest x2 59.2 us: from_everyone(): return lax.all_to_all(copies, axis, split_axis=0, concat_axis=0, tiled=True)]
    all_to_all x1 -> x0, waiting for transfers between devices: 26.3 us -> none  [sum_at_owner(): tiles = lax.all_to_all(cut_along(array, dim, count), axis, 0, 0, tiled=True)]
    all_to_all x1 -> x0, starting transfers between devices: 24.4 us -> none  [sum_at_owner(): tiles = lax.all_to_all(cut_along(array, dim, count), axis, 0, 0, tiled=True)]
    dot_general x4 -> x0, matrix products: 17.8 us -> none  [the longest x2 13.3 us: rounded_partial(): lax.dot_general(left, right_t, (((1,), (1,)), ((), ())), preferred_elemen...]
  transfers between devices with their start and end apart: 2 -> 0, of which waited for: 2 -> 0; matrix products, arithmetic and copies ran while one was open for 0% -> 0% of each run, Pallas kernels for 0% -> 0%
where the time goes in v1:
time: 118 us
  Pallas kernels  114 us (97%)
  local copies, waits for them, and re-layouts  3.16 us (3%)
    pallas_call x1, Pallas kernels, local(): pl.pallas_call(layer_kernel, out_shape=jax.ShapeDtypeStruct((SEQ, WIDTH),...  114 us
    unnamed x1, local copies, waits for them, and re-layouts  3.16 us

profile of v1, /device:TPU:1, one launch (start us, length us, event | category | flops | bytes accessed | tf_op | source)
XLA Modules:
  0.0 117.5 jit_solution(15793241511950253545)
XLA Ops:
  0.0 114.3 %shard_map.118 = bf16[512,2048]{1,0:T(8,128)(2,1)} custom-call(bf16[512,2048]{1,0:T(8,128)(2,1)} %tok_hbm.1, bf16[64,128]{1,0:T(8,128)(2,1)} %go_hbm.1, bf16[64,128]{1,0:T(8,128)(2,1)} %gi_hbm.1, bf16[64,128]{1,0:T(8,128)(2,1)} %ci_hbm.1, bf16[64,128]{1,0:T(8,128)(2,1)} %mo_hbm.1, bf16[64,1024]{1,0:T(8,128)(2,1)} %up_hbm.1, bf16[64,1024]{1,0:T(8,128)(2,1)} %dn_hbm.1, ...), custom_call_target="tpu_custom_call" | custom-call | tf_op jit(solution)/shard_map/pallas_call | solution.py:403
  114.4 3.2 %copy.14 = bf16[512,2048]{1,0:T(8,128)(2,1)} copy(bf16[512,2048]{1,0:T(8,128)(2,1)} %shard_map.118) | data formatting | bytes 4194304

commit v2 on v1

--- a/solution.py
+++ b/solution.py
@@ -14,12 +14,23 @@
 SEQ, WIDTH = 512, 2048
 ROWS = 64
 GROUP = 256
-CHUNKS, CHUNK = 8, 256
+PARTS = 2
+PART = SEQ // PARTS
+CORE_ROWS, OWN = PART // 2, PART // 8
+CHUNKS, CHUNK = 4, 512
 ARRIVAL = (0, 1, -1, 2, -2, 3, -3, 4)
 
 LINK_RATE, LINK_LAT = 46.6e3, 1.9
 PAIR_RATE, PAIR_LAT = 500e3, 1.1
 BACKLOG = 1.0
+
+
+PIECES = (
+    ("m0", "y", 128, 1), ("m1", "y", 128, 1), ("m2", "z", 256, 1),
+    ("u0", "y", 128, 4), ("u1", "y", 256, 4), ("u2", "z", 384, 4), ("u3", "z", 256, 4),
+    ("d0", "y", 128, 5), ("d1", "y", 256, 5), ("d2", "z", 384, 5), ("d3", "z", 256, 5),
+)
+NOT_BEFORE = {4: 0.0, 5: 0.0}
 
 
 class Op:
@@ -37,15 +48,16 @@
         for at, op in enumerate(left):
             if any(d not in done for d in op.deps):
                 continue
-            ready = max([done[d] for d in op.deps], default=0.0)
+            ready = max([done[d] for d in op.deps], default=NOT_BEFORE.get(op.prio, 0.0))
+            ready = max(ready, NOT_BEFORE.get(op.prio, 0.0))
             if op.link is not None:
-                ready = max(ready, link_free.get(op.link, 0.0) - BACKLOG)
+                ready = max(ready, link_free.get(op.link, 0.0) - (BACKLOG if op.prio >= 3 else 3 * BACKLOG))
             key = (max(ready, now), op.prio, at)
             if best is None or key < best[0]:
                 best = (key, op)
         (start, _, _), op = best
         left.remove(op)
-        now = start + (op.dur if op.link is None else 0.02)
+        now = start + (op.dur if op.link is None else 0.03)
         if op.link is None:
             done[op.name] = now + op.latency
         else:
@@ -60,7 +72,7 @@
 def layer_kernel(
     tok_hbm, go_hbm, gi_hbm, ci_hbm, mo_hbm, up_hbm, dn_hbm, taps, mgain, mshift, cgain, cshift,
     out_hbm,
-    tok, wm, wu, wd, proj, prod, conv, ps, so, dr, rl, fr, fd, v, first, hid, res,
+    tok, wm, wu, wd, proj, prod, conv, pp, so, dr, rl, fr, fd, v, first, hid, res,
     send_sems, recv_sems, load_sems, store_sems,
     report=None,
 ):
@@ -189,22 +201,33 @@
             names = here + [f"{tag}.Y{h}{d}{dist}" for h in (1, 2) for d in "+-"]
             ready[tag[0], dist] = ready.get((tag[0], dist), []) + names
 
+    seen = []
     mixer_loads = ["load.m0", "load.m1", "load.m2", "load.m3"]
-    y_first("my", wm, 0, 256, ["load.m0", "load.m1"], 1)
-    z_first("mz", wm, 256, 256, ["load.m2", "load.m3"], 1)
-    y_first("uy", wu, 0, 384, ["load.u"], 3)
-    z_first("uz", wu, 384, 640, ["load.u"], 3)
-    y_first("dy", wd, 0, 384, ["load.d"], 5)
-    z_first("dz", wd, 384, 640, ["load.d"], 5)
-
-    def project():
-        def step(i, _):
-            rows = pl.ds(pl.multiple_of(i * 128, 128), 128)
-            proj[rows, :] = jnp.dot(
-                tok[rows, :], wm[:, :, 0:384].reshape(WIDTH, 384), preferred_element_type=f32)
-            return 0
-
-        lax.fori_loop(0, SEQ // 128, step, 0)
+    column, loads_of = 0, {"m": mixer_loads, "u": ["load.u"], "d": ["load.d"]}
+    for tag, way, n, prio in PIECES:
+        w = {"m": wm, "u": wu, "d": wd}[tag[0]]
+        if tag[0] not in [t[0] for t in seen]:
+            column = 0
+        seen.append(tag)
+        way = y_first if way == "y" else z_first
+        way(tag, w, column, n, loads_of[tag[0]], prio)
+        column += n
+
+    def project(first_one, dists):
+        def emit():
+            for at, dist in enumerate(dists):
+                g = mod(zl + dist, NZ)
+                term = jnp.dot(
+                    tok[:, pl.ds(pl.multiple_of(g * GROUP, GROUP), GROUP)], wm[g, :, 0:384],
+                    preferred_element_type=f32)
+                if first_one and at == 0:
+                    proj[...] = term
+                else:
+                    proj[...] += term
+
+        return emit
+
+    def convolve():
         prod[0:8, :] = jnp.zeros((8, 128), f32)
         prod[8:, :] = proj[:, 128:256] * proj[:, 256:384]
         total = taps[0:1, :] * prod[6:6 + SEQ, :]
@@ -212,150 +235,145 @@
         total = total + taps[2:3, :] * prod[8:8 + SEQ, :]
         conv[...] = (proj[:, 0:128] * total).astype(bf16)
 
-    mixer_ready = [n for dist in ARRIVAL for n in ready["m", dist]]
-    compute("project", ["load.t"] + mixer_loads + mixer_ready, project, 0, 3.0)
-
-    half_rows = lambda which: pl.ds(pl.multiple_of(which * GROUP, GROUP), GROUP)
+    compute_after = ["load.t"] + mixer_loads
+    for dist in ARRIVAL:
+        compute_after = compute_after + ready["m", dist]
+        compute(f"project{dist}", compute_after, project(dist == 0, [dist]), 0, 0.35)
+        compute_after = [f"project{dist}"]
+    compute("convolve", compute_after, convolve, 0, 0.7)
+
     nt = (((1,), (1,)), ((), ()))
 
-    def product(phase, k, left, right):
-        weight = right()
-        ps[phase, k] = lax.dot_general(
-            left[half_rows(1 - c), :], weight, nt, preferred_element_type=f32).astype(bf16)
-        so[phase, k] = lax.dot_general(
-            left[half_rows(c), :], weight, nt, preferred_element_type=f32).astype(bf16)
+    def product(phase, p, k, left, rights):
+        for at, right in enumerate(rights):
+            pp[phase, p, k, :, at * GROUP:(at + 1) * GROUP] = lax.dot_general(
+                left[p * PART:(p + 1) * PART, :], right(), nt, preferred_element_type=f32).astype(bf16)
 
     def rows_of(dx):
-        return pl.ds(pl.multiple_of(mod(x + dx, NX) * ROWS, ROWS), ROWS)
-
-    def own_rows():
-        return pl.ds(pl.multiple_of((c * NX + x) * ROWS, ROWS), ROWS)
-
-    def sum_chunk(phase, k, column, residual, prio):
-        t = f"s{phase}.{k}"
+        return pl.ds(pl.multiple_of(mod(x + dx, NX) * OWN, OWN), OWN)
+
+    def core_rows(core):
+        return pl.ds(pl.multiple_of(core * CORE_ROWS, CORE_ROWS), CORE_ROWS)
+
+    def seq_rows(p, dx=0, core=None):
+        core = c if core is None else core
+        return pl.ds(pl.multiple_of(p * PART + core * CORE_ROWS + mod(x + dx, NX) * OWN, OWN), OWN)
+
+    def sum_chunk(phase, p, k, groups, residual, prio):
+        t = f"s{phase}{p}.{k}"
         d, e = ("+", "-") if k % 2 == 0 else ("-", "+")
         s = sign[d]
-        send(f"{t}.pair", "c", [f"{t}.product"], lambda: ps.at[phase, k], lambda: dr.at[phase, k],
-             lambda: dr.at[phase, k], GROUP * CHUNK * 2, prio)
+        send(f"{t}.pair", "c", [f"{t}.product"], lambda: pp.at[phase, p, k, core_rows(1 - c), :],
+             lambda: dr.at[phase, p, k], lambda: dr.at[phase, p, k], CORE_ROWS * CHUNK * 2, prio)
 
         def add_pair():
-            so[phase, k] = (so[phase, k].astype(f32) + dr[phase, k].astype(f32)).astype(bf16)
-
-        compute(f"{t}.add", [f"{t}.product", f"{t}.pair"], add_pair, prio, 0.15)
-        size = ROWS * CHUNK * 2
-        at = lambda dx: (lambda: so.at[phase, k, rows_of(dx), :])
-        slot = lambda ref: (lambda: ref.at[phase, k])
+            so[phase, p, k] = (
+                pp[phase, p, k, core_rows(c), :].astype(f32) + dr[phase, p, k].astype(f32)).astype(bf16)
+
+        compute(f"{t}.add", [f"{t}.product", f"{t}.pair"], add_pair, prio, 0.06)
+        size = OWN * CHUNK * 2
+        at = lambda dx: (lambda: so.at[phase, p, k, rows_of(dx), :])
+        slot = lambda ref: (lambda: ref.at[phase, p, k])
         send(f"{t}.relay", "x" + d, [f"{t}.add"], at(2), slot(rl), slot(rl), size, prio)
-        send(f"{t}.direct", "x" + e, [f"{t}.add"], at(-s), slot(fd), slot(fd), size, prio)
+        send(f"{t}.direct", "x" + e, [f"{t}.add"], at(-s), slot(fd), slot(fd), size, prio + 0.5)
 
         def add_relay():
-            so[phase, k, rows_of(s), :] = (
-                so[phase, k, rows_of(s), :].astype(f32) + rl[phase, k].astype(f32)).astype(bf16)
-
-        compute(f"{t}.radd", [f"{t}.add", f"{t}.relay"], add_relay, prio, 0.05)
+            so[phase, p, k, rows_of(s), :] = (
+                so[phase, p, k, rows_of(s), :].astype(f32) + rl[phase, p, k].astype(f32)).astype(bf16)
+
+        compute(f"{t}.radd", [f"{t}.add", f"{t}.relay"], add_relay, prio, 0.03)
         send(f"{t}.final", "x" + d, [f"{t}.radd"], at(s), slot(fr), slot(fr), size, prio)
 
         def finish():
-            columns = pl.ds(pl.multiple_of(column() * CHUNK, CHUNK), CHUNK)
-            total = so[phase, k, rows_of(0), :].astype(f32) + fr[phase, k].astype(f32)
-            total = total + fd[phase, k].astype(f32)
-            v[:, columns] = residual_scale * residual[own_rows(), columns].astype(f32) + total
-
-        compute(f"{t}.finish", [f"{t}.add", f"{t}.final", f"{t}.direct"], finish, prio, 0.05)
-
-    def norm(phase, gain, shift, dest):
+            total = so[phase, p, k, rows_of(0), :].astype(f32) + fr[phase, p, k].astype(f32)
+            total = total + fd[phase, p, k].astype(f32)
+            for at, group in enumerate(groups):
+                columns = pl.ds(pl.multiple_of(group() * GROUP, GROUP), GROUP)
+                v[p, :, columns] = (residual_scale * residual[seq_rows(p), columns].astype(f32)
+                                    + total[:, at * GROUP:(at + 1) * GROUP])
+
+        compute(f"{t}.finish", [f"{t}.add", f"{t}.final", f"{t}.direct"], finish, prio, 0.04)
+
+    def norm(phase, p, gain, shift, dest, prio):
         def emit():
-            values = v[...]
+            values = v[p]
             mean = jnp.mean(values, -1, keepdims=True)
             centered = values - mean
             variance = jnp.mean(centered * centered, -1, keepdims=True)
             scaled = centered * lax.rsqrt(variance + norm_epsilon)
-            dest[own_rows(), :] = (scaled * gain[...] + shift[...]).astype(bf16)
-
-        compute(f"norm{phase}", [f"s{phase}.{k}.finish" for k in range(CHUNKS)], emit, 0, 0.7)
+            dest[seq_rows(p), :] = (scaled * gain[...] + shift[...]).astype(bf16)
+
+        compute(f"norm{phase}{p}", [f"s{phase}{p}.{k}.finish" for k in range(CHUNKS)], emit, prio, 0.25)
 
     HALF = WIDTH // 2
 
-    def gather(phase, ref):
-        def at(dx, h, other=False):
-            def view():
-                core = 1 - c if other else c
-                rows = pl.ds(pl.multiple_of((core * NX + mod(x + dx, NX)) * ROWS, ROWS), ROWS)
-                return ref.at[rows, :] if h is None else ref.at[rows, pl.ds(h * HALF, HALF)]
-            return view
-
-        t, size, landed = f"g{phase}", ROWS * HALF * 2, []
-        start = [f"norm{phase}"]
+    def place(p, dx, h, other=False):
+        def view(ref):
+            rows = seq_rows(p, dx, 1 - c if other else c)
+            return ref.at[rows, :] if h is None else ref.at[rows, pl.ds(h * HALF, HALF)]
+        return view
+
+    def gather(phase, p, ref, prio):
+        def at(*where):
+            return lambda: place(p, *where)(ref)
+
+        t, size, landed = f"g{phase}{p}", OWN * HALF * 2, []
+        start = [f"norm{phase}{p}"]
         for d, first_half in (("+", 0), ("-", 1)):
             for h in (first_half, 1 - first_half):
-                send(f"{t}.A{d}{h}", "x" + d, start, at(0, h), at(0, h), at(-sign[d], h), size, 0)
-                landed.append((f"{t}.A{d}{h}", at(-sign[d], h)))
-        send(f"{t}.P", "c", start, at(0, None), at(0, None), at(0, None, True), 2 * size, 0)
-        landed.append((f"{t}.P", at(0, None, True)))
+                send(f"{t}.A{d}{h}", "x" + d, start, at(0, h), at(0, h), at(-sign[d], h), size, prio)
+                landed.append((f"{t}.A{d}{h}", (-sign[d], h)))
+        send(f"{t}.P", "c", start, at(0, None), at(0, None), at(0, None, True), 2 * size, prio)
+        landed.append((f"{t}.P", (0, None, True)))
         for d, h in (("+", 0), ("-", 1)):
             b = at(-sign[d], h)
-            send(f"{t}.B{d}", "x" + d, [f"{t}.A{d}{h}"], b, b, at(2, h), size, 0)
-            landed.append((f"{t}.B{d}", at(2, h)))
+            send(f"{t}.B{d}", "x" + d, [f"{t}.A{d}{h}"], b, b, at(2, h), size, prio)
+            landed.append((f"{t}.B{d}", (2, h)))
         for name, dx, h in ((f"{t}.A+0", -1, 0), (f"{t}.A-1", 1, 1), (f"{t}.A+1", -1, 1),
                             (f"{t}.A-0", 1, 0), (f"{t}.B+", 2, 0), (f"{t}.B-", 2, 1)):
-            send(f"{name}.P", "c", [name], at(dx, h), at(dx, h), at(dx, h, True), size, 0)
-            landed.append((f"{name}.P", at(dx, h, True)))
-        return landed, at(0, None)
-
-    for k in range(CHUNKS):
-        compute(f"s0.{k}.product", ["project"],
-                functools.partial(product, 0, k, conv, lambda k=k: wm[k, :, 384:512]), 1, 0.25)
-        sum_chunk(0, k, lambda k=k: k, tok, 0)
-    norm(0, mgain, mshift, first)
-    landed0, _ = gather(0, first)
-
-    def hidden(n):
+            send(f"{name}.P", "c", [name], at(dx, h), at(dx, h), at(dx, h, True), size, prio)
+            landed.append((f"{name}.P", (dx, h, True)))
+        return landed
+
+    def hidden(p, n):
         columns = pl.ds(n * 256, 256)
-        for r in range(2):
-            rows = pl.ds(r * 256, 256)
-            up = jnp.dot(first[rows, :], wu[:, :, columns].reshape(WIDTH, 256), preferred_element_type=f32)
-            hid[rows, columns] = jnp.square(jnp.maximum(up, 0.0)).astype(bf16)
+        rows = pl.ds(p * PART, PART)
+        up = jnp.dot(first[rows, :], wu[:, :, columns].reshape(WIDTH, 256), preferred_element_type=f32)
+        hid[rows, columns] = jnp.square(jnp.maximum(up, 0.0)).astype(bf16)
+
+    stores = []
+
+    def store(name, deps, where):
+        index = len(stores)
+        copy = lambda: pltpu.make_async_copy(where(res), where(out_hbm), store_sems.at[index])
+        stores.append(copy)
+        ops.append(Op(name, deps, lambda: copy().start(), 5, dur=0.02))
 
     up_ready = ["load.u"] + [n for dist in ARRIVAL for n in ready["u", dist]]
-    for n in range(4):
-        compute(f"hidden{n}", ["norm0"] + [name for name, _ in landed0] + up_ready,
-                functools.partial(hidden, n), 2, 1.0)
-    for k, dist in enumerate(ARRIVAL):
-        group = lambda dist=dist: mod(zl + dist, NZ)
-        compute(f"s1.{k}.product", [f"hidden{n}" for n in range(4)] + ["load.d"] + ready["d", dist],
-                functools.partial(product, 1, k, hid, lambda group=group: wd[group()]), 1, 0.6)
-        sum_chunk(1, k, group, first, 0)
-    norm(1, cgain, cshift, res)
-    landed1, mine = gather(1, res)
-
-    stores = []
-
-    def store(name, deps, view):
-        index = len(stores)
-
-        def copy():
-            source = view()
-            return pltpu.make_async_copy(source, out_view(view), store_sems.at[index])
-
-        stores.append(copy)
-        ops.append(Op(name, deps, lambda: copy().start(), 2, dur=0.02))
-
-    def out_view(view):
-        return view(out_hbm)
-
-    def place(dx, h, other):
-        def view(ref=res):
-            core = 1 - c if other else c
-            rows = pl.ds(pl.multiple_of((core * NX + mod(x + dx, NX)) * ROWS, ROWS), ROWS)
-            return ref.at[rows, :] if h is None else ref.at[rows, pl.ds(h * HALF, HALF)]
-        return view
-
-    store("out.own", ["norm1"], place(0, None, False))
-    store("out.P", ["g1.P"], place(0, None, True))
-    for name, dx, h in (("g1.A+0", -1, 0), ("g1.A-1", 1, 1), ("g1.A+1", -1, 1),
-                        ("g1.A-0", 1, 0), ("g1.B+", 2, 0), ("g1.B-", 2, 1)):
-        store(f"out.{name}", [name], place(dx, h, False))
-        store(f"out.{name}.P", [f"{name}.P"], place(dx, h, True))
+    for p in range(PARTS):
+        for k in range(CHUNKS):
+            pair = (2 * k, 2 * k + 1)
+            compute(f"s0{p}.{k}.product", ["convolve"],
+                    functools.partial(product, 0, p, k, conv, [lambda g=g: wm[g, :, 384:512] for g in pair]),
+                    0 + p, 0.25)
+            sum_chunk(0, p, k, [lambda g=g: g for g in pair], tok, 0 + p)
+        norm(0, p, mgain, mshift, first, 0 + p)
+        landed = gather(0, p, first, 0 + p)
+        for n in range(4):
+            compute(f"hidden{p}{n}", [f"norm0{p}"] + [name for name, _ in landed] + up_ready,
+                    functools.partial(hidden, p, n), 2 + p, 0.37)
+        for k in range(CHUNKS):
+            dists = ARRIVAL[2 * k:2 * k + 2]
+            groups = [lambda dist=dist: mod(zl + dist, NZ) for dist in dists]
+            arrived = [name for dist in dists for name in ready["d", dist]]
+            compute(f"s1{p}.{k}.product", [f"hidden{p}{n}" for n in range(4)] + ["load.d"] + arrived,
+                    functools.partial(product, 1, p, k, hid, [lambda g=g: wd[g()] for g in groups]),
+                    2 + p, 0.5)
+            sum_chunk(1, p, k, groups, first, 2 + p)
+        norm(1, p, cgain, cshift, res, 2 + p)
+        store(f"out{p}.own", [f"norm1{p}"], place(p, 0, None))
+        for name, where in gather(1, p, res, 2 + p):
+            store(f"out.{name}", [name], place(p, *where))
 
     order, done = plan(ops)
     if report is not None:
@@ -389,11 +407,7 @@
         copy().wait()
 
 
-N_SENDS, N_LOADS, N_STORES = 256, 7, 14
-
-
-def count_ops():
-    return N_SENDS, N_LOADS, N_STORES
+N_SENDS, N_LOADS, N_STORES = 480, 7, 28
 
 
 def local(tokens, gate_outer, gate_inner, conv_input, mixer_output, conv_taps, mixer_gain,
@@ -413,13 +427,13 @@
             pltpu.VMEM((SEQ, 384), f32),
             pltpu.VMEM((SEQ + 8, 128), f32),
             pltpu.VMEM((SEQ, 128), bf16),
-            pltpu.VMEM((2, CHUNKS, GROUP, CHUNK), bf16),
-            pltpu.VMEM((2, CHUNKS, GROUP, CHUNK), bf16),
-            pltpu.VMEM((2, CHUNKS, GROUP, CHUNK), bf16),
-            pltpu.VMEM((2, CHUNKS, ROWS, CHUNK), bf16),
-            pltpu.VMEM((2, CHUNKS, ROWS, CHUNK), bf16),
-            pltpu.VMEM((2, CHUNKS, ROWS, CHUNK), bf16),
-            pltpu.VMEM((ROWS, WIDTH), f32),
+            pltpu.VMEM((2, PARTS, CHUNKS, PART, CHUNK), bf16),
+            pltpu.VMEM((2, PARTS, CHUNKS, CORE_ROWS, CHUNK), bf16),
+            pltpu.VMEM((2, PARTS, CHUNKS, CORE_ROWS, CHUNK), bf16),
+            pltpu.VMEM((2, PARTS, CHUNKS, OWN, CHUNK), bf16),
+            pltpu.VMEM((2, PARTS, CHUNKS, OWN, CHUNK), bf16),
+            pltpu.VMEM((2, PARTS, CHUNKS, OWN, CHUNK), bf16),
+            pltpu.VMEM((PARTS, OWN, WIDTH), f32),
             pltpu.VMEM((SEQ, WIDTH), bf16),
             pltpu.VMEM((SEQ, 1024), bf16),
             pltpu.VMEM((SEQ, WIDTH), bf16),

time: 118 us -> 116 us (0.983)
    pallas_call x1, Pallas kernels: 114 us -> 113 us  [local(): pl.pallas_call(layer_kernel, out_shape=jax.ShapeDtypeStruct((SEQ, WIDTH),...]
where the time goes in v2:
time: 116 us
  Pallas kernels  113 us (97%)
  local copies, waits for them, and re-layouts  3.16 us (3%)
    pallas_call x1, Pallas kernels, local(): pl.pallas_call(layer_kernel, out_shape=jax.ShapeDtypeStruct((SEQ, WIDTH),...  113 us
    unnamed x1, local copies, waits for them, and re-layouts  3.16 us

profile of v2, /device:TPU:1, one launch (start us, length us, event | category | flops | bytes accessed | tf_op | source)
XLA Modules:
  0.0 115.7 jit_solution(7713479624147528094)
XLA Ops:
  0.0 112.5 %shard_map.118 = bf16[512,2048]{1,0:T(8,128)(2,1)} custom-call(bf16[512,2048]{1,0:T(8,128)(2,1)} %tok_hbm.1, bf16[64,128]{1,0:T(8,128)(2,1)} %go_hbm.1, bf16[64,128]{1,0:T(8,128)(2,1)} %gi_hbm.1, bf16[64,128]{1,0:T(8,128)(2,1)} %ci_hbm.1, bf16[64,128]{1,0:T(8,128)(2,1)} %mo_hbm.1, bf16[64,1024]{1,0:T(8,128)(2,1)} %up_hbm.1, bf16[64,1024]{1,0:T(8,128)(2,1)} %dn_hbm.1, ...), custom_call_target="tpu_custom_call" | custom-call | tf_op jit(solution)/shard_map/pallas_call | solution.py:417
  112.5 3.2 %copy.14 = bf16[512,2048]{1,0:T(8,128)(2,1)} copy(bf16[512,2048]{1,0:T(8,128)(2,1)} %shard_map.118) | data formatting | bytes 4194304

commit v3 on v2

--- a/solution.py
+++ b/solution.py
@@ -31,17 +31,25 @@
     ("d0", "y", 128, 5), ("d1", "y", 256, 5), ("d2", "z", 384, 5), ("d3", "z", 256, 5),
 )
 NOT_BEFORE = {4: 0.0, 5: 0.0}
+PRIORITY = {}
 
 
 class Op:
     def __init__(self, name, deps, emit, prio, dur=0.0, link=None, nbytes=0, wait=None, latency=0.0):
         self.name, self.deps, self.emit, self.prio = name, deps, emit, prio
         self.dur, self.link, self.nbytes, self.wait = dur, link, nbytes, wait
-        self.latency = latency
+        self.latency, self.group = latency, None
 
 
 def plan(ops):
     done, link_free, order, now = {}, {}, [], 0.0
+    members = {}
+    for op in ops:
+        if op.group is not None:
+            members.setdefault(op.group, []).append(op.name)
+    group_of = {op.name: members[op.group] for op in ops if op.group is not None}
+    for op in ops:
+        op.deps = list(dict.fromkeys(m for d in op.deps for m in group_of.get(d, [d])))
     left = list(ops)
     while left:
         best = None
@@ -71,9 +79,9 @@
 
 def layer_kernel(
     tok_hbm, go_hbm, gi_hbm, ci_hbm, mo_hbm, up_hbm, dn_hbm, taps, mgain, mshift, cgain, cshift,
-    out_hbm,
-    tok, wm, wu, wd, proj, prod, conv, pp, so, dr, rl, fr, fd, v, first, hid, res,
-    send_sems, recv_sems, load_sems, store_sems,
+    res,
+    tok, wm, wu, wd, proj, prod, conv, pp, so, dr, rl, fr, fd, v, first, hid,
+    send_sems, recv_sems, load_sems,
     report=None,
 ):
     f32, bf16 = jnp.float32, jnp.bfloat16
@@ -100,22 +108,28 @@
     sign = {"+": 1, "-": -1}
 
     ops = []
-    sends = []
-
-    def send(name, link, deps, src, dst, landed, nbytes, prio):
-        index = len(sends)
+    sends = {}
+
+    send_groups, recv_groups = {}, {}
+
+    def send(name, link, deps, src, dst, landed, nbytes, prio, sent, group=None):
+        send_at = send_groups.setdefault(sent[0], len(send_groups))
+        recv_at = recv_groups.setdefault(group[0] if group else name, len(recv_groups))
 
         def copy(s, d):
             return pltpu.make_async_remote_copy(
-                src_ref=s, dst_ref=d, send_sem=send_sems.at[index], recv_sem=recv_sems.at[index],
+                src_ref=s, dst_ref=d, send_sem=send_sems.at[send_at], recv_sem=recv_sems.at[recv_at],
                 device_id=peer[link], device_id_type=pl.DeviceIdType.MESH,
             )
 
-        sends.append((name, lambda: copy(src(), dst()).wait_send()))
-        ops.append(Op(
+        all_here = group[1] if group else landed
+        sends.setdefault(sent[0], lambda: copy(sent[1](), sent[1]()).wait_send())
+        op = Op(
             name, deps, lambda: copy(src(), dst()).start(), prio, link=link, nbytes=nbytes,
-            wait=lambda: copy(landed(), landed()).wait_recv(),
-        ))
+            wait=lambda: copy(all_here(), all_here()).wait_recv(),
+        )
+        op.group = group[0] if group else None
+        ops.append(op)
 
     def compute(name, deps, emit, prio, dur):
         ops.append(Op(name, deps, emit, prio, dur=dur))
@@ -157,14 +171,21 @@
 
     def y_first(tag, w, c0, n, deps, prio):
         size = ROWS * n * 2
+        part_of = lambda zs, rows: (lambda: w.at[zs, rows, pl.ds(c0, n)])
+        sent_y = (f"{tag}.Y", part_of(0, pl.ds(0, 3 * ROWS)))
+        sent_z = (f"{tag}.Z", part_of(pl.ds(0, 7), pl.ds(0, GROUP)))
+        second = (f"{tag}.Y2", part_of(0, pl.ds(0, ROWS)))
+        fourth = (f"{tag}.Z4", part_of(0, pl.ds(0, GROUP)))
         for d in "+-":
             s = sign[d]
             b = block(w, 0, 0, c0, n)
-            send(f"{tag}.Y1{d}", "y" + d, deps, b, b, block(w, 0, -s, c0, n), size, prio)
+            send(f"{tag}.Y1{d}", "y" + d, deps, b, b, block(w, 0, -s, c0, n), size,
+                 PRIORITY.get(f"{tag[0]}yY1", prio), sent_y)
         for d, half in (("+", 0), ("-", 1)):
             s = sign[d]
             b = block(w, 0, -s, c0, n, half)
-            send(f"{tag}.Y2{d}", "y" + d, [f"{tag}.Y1{d}"], b, b, block(w, 0, -2 * s, c0, n, half), size // 2, prio)
+            send(f"{tag}.Y2{d}", "y" + d, [f"{tag}.Y1{d}"], b, b, block(w, 0, -2 * s, c0, n, half), size // 2,
+                 PRIORITY.get(f"{tag[0]}yY2", prio), sent_y, second)
         group = [f"{tag}.Y{h}{d}" for h in (1, 2) for d in "+-"]
         ready[tag[0], 0] = ready.get((tag[0], 0), []) + group
         for d, half in (("+", 0), ("-", 1)):
@@ -174,12 +195,17 @@
                 b = slab(w, -s * (h - 1), c0, n, part)
                 before = deps + group if h == 1 else [f"{tag}.Z{h - 1}{d}"]
                 send(f"{tag}.Z{h}{d}", "z" + d, before, b, b, slab(w, -s * h, c0, n, part),
-                     NY * size // (1 if part is None else 2), prio)
+                     NY * size // (1 if part is None else 2), PRIORITY.get(f"{tag[0]}yZ{h}", prio),
+                     sent_z, fourth if h == 4 else None)
                 dist = 4 if h == 4 else -s * h
                 ready[tag[0], dist] = ready.get((tag[0], dist), []) + [f"{tag}.Z{h}{d}"]
 
     def z_first(tag, w, c0, n, deps, prio):
         size = ROWS * n * 2
+        part_of = lambda zs, rows: (lambda: w.at[zs, rows, pl.ds(c0, n)])
+        sent_z = part_of(0, pl.ds(0, 7 * ROWS // 2))
+        sent_y = (f"{tag}.Y", part_of(pl.ds(0, 6), pl.ds(0, GROUP)))
+        fourth = (f"{tag}.Z4", part_of(0, pl.ds(0, ROWS)))
         for d, half in (("+", 0), ("-", 1)):
             s = sign[d]
             for h in (1, 2, 3, 4):
@@ -187,17 +213,25 @@
                 b = block(w, -s * (h - 1), 0, c0, n, part)
                 before = deps if h == 1 else [f"{tag}.Z{h - 1}{d}"]
                 send(f"{tag}.Z{h}{d}", "z" + d, before, b, b, block(w, -s * h, 0, c0, n, part),
-                     size // (1 if part is None else 2), prio)
-        for dist in ARRIVAL:
+                     size // (1 if part is None else 2), PRIORITY.get(f"{tag[0]}zZ{h}", prio),
+                     (f"{tag}.Z{d}", sent_z), fourth if h == 4 else None)
+        for at, dist in enumerate(ARRIVAL):
             here = {0: deps, 4: [f"{tag}.Z4+", f"{tag}.Z4-"]}.get(
                 dist, [f"{tag}.Z{abs(dist)}{'-' if dist > 0 else '+'}"])
+            second = {
+                "m": (f"{tag}.Y2.{at}", part_of(0, pl.ds(0, ROWS))),
+                "u": (f"{tag}.Y2", part_of(pl.ds(0, 2), pl.ds(0, GROUP))),
+                "d": (f"{tag}.Y2.{at // 2}", part_of(0, pl.ds(0, 2 * ROWS))),
+            }[tag[0]]
             for d, half in (("+", 0), ("-", 1)):
                 s = sign[d]
                 b = block(w, dist, 0, c0, n)
-                send(f"{tag}.Y1{d}{dist}", "y" + d, here, b, b, block(w, dist, -s, c0, n), size, prio)
+                send(f"{tag}.Y1{d}{dist}", "y" + d, here, b, b, block(w, dist, -s, c0, n), size,
+                     PRIORITY.get(f"{tag[0]}zY{abs(dist)}", prio), sent_y)
                 b = block(w, dist, -s, c0, n, half)
                 send(f"{tag}.Y2{d}{dist}", "y" + d, [f"{tag}.Y1{d}{dist}"], b, b,
-                     block(w, dist, -2 * s, c0, n, half), size // 2, prio)
+                     block(w, dist, -2 * s, c0, n, half), size // 2,
+                     PRIORITY.get(f"{tag[0]}zY{abs(dist)}", prio), sent_y, second)
             names = here + [f"{tag}.Y{h}{d}{dist}" for h in (1, 2) for d in "+-"]
             ready[tag[0], dist] = ready.get((tag[0], dist), []) + names
 
@@ -264,7 +298,8 @@
         d, e = ("+", "-") if k % 2 == 0 else ("-", "+")
         s = sign[d]
         send(f"{t}.pair", "c", [f"{t}.product"], lambda: pp.at[phase, p, k, core_rows(1 - c), :],
-             lambda: dr.at[phase, p, k], lambda: dr.at[phase, p, k], CORE_ROWS * CHUNK * 2, prio)
+             lambda: dr.at[phase, p, k], lambda: dr.at[phase, p, k], CORE_ROWS * CHUNK * 2, prio,
+             (f"s{phase}{p}.pair", lambda: dr.at[phase, p]))
 
         def add_pair():
             so[phase, p, k] = (
@@ -274,15 +309,18 @@
         size = OWN * CHUNK * 2
         at = lambda dx: (lambda: so.at[phase, p, k, rows_of(dx), :])
         slot = lambda ref: (lambda: ref.at[phase, p, k])
-        send(f"{t}.relay", "x" + d, [f"{t}.add"], at(2), slot(rl), slot(rl), size, prio)
-        send(f"{t}.direct", "x" + e, [f"{t}.add"], at(-s), slot(fd), slot(fd), size, prio + 0.5)
+        sent = (f"s{phase}{p}.x", lambda: so.at[phase, p, pl.ds(0, CHUNKS - 1)])
+        last = (f"{t}.last", lambda: so.at[phase, p, k, pl.ds(0, 2 * OWN), :])
+        send(f"{t}.relay", "x" + d, [f"{t}.add"], at(2), slot(rl), slot(rl), size, prio, sent)
+        send(f"{t}.direct", "x" + e, [f"{t}.add"], at(-s), slot(fd), slot(fd), size, prio + 0.5,
+             sent, last)
 
         def add_relay():
             so[phase, p, k, rows_of(s), :] = (
                 so[phase, p, k, rows_of(s), :].astype(f32) + rl[phase, p, k].astype(f32)).astype(bf16)
 
         compute(f"{t}.radd", [f"{t}.add", f"{t}.relay"], add_relay, prio, 0.03)
-        send(f"{t}.final", "x" + d, [f"{t}.radd"], at(s), slot(fr), slot(fr), size, prio)
+        send(f"{t}.final", "x" + d, [f"{t}.radd"], at(s), slot(fr), slot(fr), size, prio, sent, last)
 
         def finish():
             total = so[phase, p, k, rows_of(0), :].astype(f32) + fr[phase, p, k].astype(f32)
@@ -319,35 +357,36 @@
 
         t, size, landed = f"g{phase}{p}", OWN * HALF * 2, []
         start = [f"norm{phase}{p}"]
+        first_rows = lambda rows: (lambda: ref.at[pl.ds(0, rows), :])
+        sent_x, sent_c = (f"{t}.x", first_rows(3 * OWN)), (f"{t}.c", first_rows(4 * OWN))
+        if phase == 0:
+            pairs = [(f"{t}.P", first_rows(4 * OWN))] * 4
+        else:
+            pairs = [(f"{t}.P{i}", first_rows(rows)) for i, rows in enumerate((OWN, OWN, OWN, OWN))]
         for d, first_half in (("+", 0), ("-", 1)):
             for h in (first_half, 1 - first_half):
-                send(f"{t}.A{d}{h}", "x" + d, start, at(0, h), at(0, h), at(-sign[d], h), size, prio)
+                send(f"{t}.A{d}{h}", "x" + d, start, at(0, h), at(0, h), at(-sign[d], h), size, prio, sent_x)
                 landed.append((f"{t}.A{d}{h}", (-sign[d], h)))
-        send(f"{t}.P", "c", start, at(0, None), at(0, None), at(0, None, True), 2 * size, prio)
+        send(f"{t}.P", "c", start, at(0, None), at(0, None), at(0, None, True), 2 * size, prio, sent_c, pairs[0])
         landed.append((f"{t}.P", (0, None, True)))
         for d, h in (("+", 0), ("-", 1)):
             b = at(-sign[d], h)
-            send(f"{t}.B{d}", "x" + d, [f"{t}.A{d}{h}"], b, b, at(2, h), size, prio)
+            send(f"{t}.B{d}", "x" + d, [f"{t}.A{d}{h}"], b, b, at(2, h), size, prio, sent_x)
             landed.append((f"{t}.B{d}", (2, h)))
-        for name, dx, h in ((f"{t}.A+0", -1, 0), (f"{t}.A-1", 1, 1), (f"{t}.A+1", -1, 1),
-                            (f"{t}.A-0", 1, 0), (f"{t}.B+", 2, 0), (f"{t}.B-", 2, 1)):
-            send(f"{name}.P", "c", [name], at(dx, h), at(dx, h), at(dx, h, True), size, prio)
+        for i, (name, dx, h) in enumerate((
+                (f"{t}.A+0", -1, 0), (f"{t}.A-1", 1, 1), (f"{t}.A+1", -1, 1),
+                (f"{t}.A-0", 1, 0), (f"{t}.B+", 2, 0), (f"{t}.B-", 2, 1))):
+            send(f"{name}.P", "c", [name], at(dx, h), at(dx, h), at(dx, h, True), size, prio,
+                 sent_c, pairs[1 + i // 2])
             landed.append((f"{name}.P", (dx, h, True)))
         return landed
 
     def hidden(p, n):
-        columns = pl.ds(n * 256, 256)
         rows = pl.ds(p * PART, PART)
-        up = jnp.dot(first[rows, :], wu[:, :, columns].reshape(WIDTH, 256), preferred_element_type=f32)
-        hid[rows, columns] = jnp.square(jnp.maximum(up, 0.0)).astype(bf16)
-
-    stores = []
-
-    def store(name, deps, where):
-        index = len(stores)
-        copy = lambda: pltpu.make_async_copy(where(res), where(out_hbm), store_sems.at[index])
-        stores.append(copy)
-        ops.append(Op(name, deps, lambda: copy().start(), 5, dur=0.02))
+        for at in (2 * n, 2 * n + 1):
+            columns = pl.ds(at * 256, 256)
+            up = jnp.dot(first[rows, :], wu[:, :, columns].reshape(WIDTH, 256), preferred_element_type=f32)
+            hid[rows, columns] = jnp.square(jnp.maximum(up, 0.0)).astype(bf16)
 
     up_ready = ["load.u"] + [n for dist in ARRIVAL for n in ready["u", dist]]
     for p in range(PARTS):
@@ -359,25 +398,25 @@
             sum_chunk(0, p, k, [lambda g=g: g for g in pair], tok, 0 + p)
         norm(0, p, mgain, mshift, first, 0 + p)
         landed = gather(0, p, first, 0 + p)
-        for n in range(4):
+        for n in range(2):
             compute(f"hidden{p}{n}", [f"norm0{p}"] + [name for name, _ in landed] + up_ready,
-                    functools.partial(hidden, p, n), 2 + p, 0.37)
+                    functools.partial(hidden, p, n), 2 + p, 0.75)
         for k in range(CHUNKS):
             dists = ARRIVAL[2 * k:2 * k + 2]
             groups = [lambda dist=dist: mod(zl + dist, NZ) for dist in dists]
             arrived = [name for dist in dists for name in ready["d", dist]]
-            compute(f"s1{p}.{k}.product", [f"hidden{p}{n}" for n in range(4)] + ["load.d"] + arrived,
+            compute(f"s1{p}.{k}.product", [f"hidden{p}{n}" for n in range(2)] + ["load.d"] + arrived,
                     functools.partial(product, 1, p, k, hid, [lambda g=g: wd[g()] for g in groups]),
                     2 + p, 0.5)
             sum_chunk(1, p, k, groups, first, 2 + p)
         norm(1, p, cgain, cshift, res, 2 + p)
-        store(f"out{p}.own", [f"norm1{p}"], place(p, 0, None))
-        for name, where in gather(1, p, res, 2 + p):
-            store(f"out.{name}", [name], place(p, *where))
+        gather(1, p, res, 2 + p)
 
     order, done = plan(ops)
     if report is not None:
-        report(order, done, len(sends), len(loads), len(stores))
+        report(order, done, len(send_groups), len(recv_groups), len(loads))
+    assert (len(send_groups), len(recv_groups), len(loads)) == (N_SENDS, N_RECVS, N_LOADS), (
+        len(send_groups), len(recv_groups), len(loads))
 
     for start_load in loads:
         start_load()
@@ -391,8 +430,9 @@
 
     def need(name):
         op = by_name[name]
-        if op.wait is not None and name not in waited:
-            waited.add(name)
+        key = op.group or name
+        if op.wait is not None and key not in waited:
+            waited.add(key)
             op.wait()
 
     for _, op in order:
@@ -401,13 +441,11 @@
         op.emit()
     for op in ops:
         need(op.name)
-    for _, wait in sends:
+    for wait in sends.values():
         wait()
-    for copy in stores:
-        copy().wait()
-
-
-N_SENDS, N_LOADS, N_STORES = 480, 7, 28
+
+
+N_SENDS, N_RECVS, N_LOADS = 43, 275, 7
 
 
 def local(tokens, gate_outer, gate_inner, conv_input, mixer_output, conv_taps, mixer_gain,
@@ -416,9 +454,9 @@
     vmem, hbm = pl.BlockSpec(memory_space=pltpu.VMEM), pl.BlockSpec(memory_space=pl.ANY)
     return pl.pallas_call(
         layer_kernel,
-        out_shape=jax.ShapeDtypeStruct((SEQ, WIDTH), bf16),
+        out_shape=pltpu.VMEM((SEQ, WIDTH), bf16),
         in_specs=[hbm] * 7 + [vmem] * 5,
-        out_specs=hbm,
+        out_specs=vmem,
         scratch_shapes=[
             pltpu.VMEM((SEQ, WIDTH), bf16),
             pltpu.VMEM((NZ, GROUP, 512), bf16),
@@ -436,11 +474,9 @@
             pltpu.VMEM((PARTS, OWN, WIDTH), f32),
             pltpu.VMEM((SEQ, WIDTH), bf16),
             pltpu.VMEM((SEQ, 1024), bf16),
-            pltpu.VMEM((SEQ, WIDTH), bf16),
             pltpu.SemaphoreType.DMA((N_SENDS,)),
-            pltpu.SemaphoreType.DMA((N_SENDS,)),
+            pltpu.SemaphoreType.DMA((N_RECVS,)),
             pltpu.SemaphoreType.DMA((N_LOADS,)),
-            pltpu.SemaphoreType.DMA((N_STORES,)),
         ],
         compiler_params=pltpu.CompilerParams(
             collective_id=0, has_side_effects=True, vmem_limit_bytes=60 * 2**20),

time: 116 us -> 107 us (0.922)
  Pallas kernels: 113 us -> 105 us
  local copies, waits for them, and re-layouts: 3.16 us -> 1.32 us
    pallas_call x1, Pallas kernels: 113 us -> 105 us  [local(): pl.pallas_call(layer_kernel, out_shape=pltpu.VMEM((SEQ, WIDTH), bf16), in...]
    unnamed x1, local copies, waits for them, and re-layouts: 3.16 us -> 1.32 us
where the time goes in v3:
time: 107 us; the launch traced here: 106 us
  Pallas kernels  105 us (98%)
  local copies, waits for them, and re-layouts  1.32 us (1%)
    pallas_call x1, Pallas kernels, local(): pl.pallas_call(layer_kernel, out_shape=pltpu.VMEM((SEQ, WIDTH), bf16), in...  105 us

profile of v3, /device:TPU:1, one launch (start us, length us, event | category | flops | bytes accessed | tf_op | source)
XLA Modules:
  0.0 106.4 jit_solution(12704712389915683424)
XLA Ops:
  0.0 105.1 %shard_map.118 = bf16[512,2048]{1,0:T(8,128)(2,1)S(1)} custom-call(bf16[512,2048]{1,0:T(8,128)(2,1)} %tok_hbm.1, bf16[64,128]{1,0:T(8,128)(2,1)} %go_hbm.1, bf16[64,128]{1,0:T(8,128)(2,1)} %gi_hbm.1, bf16[64,128]{1,0:T(8,128)(2,1)} %ci_hbm.1, bf16[64,128]{1,0:T(8,128)(2,1)} %mo_hbm.1, bf16[64,1024]{1,0:T(8,128)(2,1)} %up_hbm.1, bf16[64,1024]{1,0:T(8,128)(2,1)} %dn_hbm.1, ...), custom_call_target="tpu_custom_call" | custom-call | tf_op jit(solution)/shard_map/pallas_call | solution.py:455
  105.1 1.3 %copy.14 = bf16[512,2048]{1,0:T(8,128)(2,1)} copy(bf16[512,2048]{1,0:T(8,128)(2,1)S(1)} %shard_map.118) | data formatting | bytes 4194304

commit v4 on v3

--- a/solution.py
+++ b/solution.py
@@ -18,20 +18,27 @@
 PART = SEQ // PARTS
 CORE_ROWS, OWN = PART // 2, PART // 8
 CHUNKS, CHUNK = 4, 512
+NEAR = ("+", "-")
 ARRIVAL = (0, 1, -1, 2, -2, 3, -3, 4)
 
 LINK_RATE, LINK_LAT = 46.6e3, 1.9
 PAIR_RATE, PAIR_LAT = 500e3, 1.1
-BACKLOG = 1.0
+BACKLOG = 1.08
 
 
 PIECES = (
-    ("m0", "y", 128, 1), ("m1", "y", 128, 1), ("m2", "z", 256, 1),
-    ("u0", "y", 128, 4), ("u1", "y", 256, 4), ("u2", "z", 384, 4), ("u3", "z", 256, 4),
-    ("d0", "y", 128, 5), ("d1", "y", 256, 5), ("d2", "z", 384, 5), ("d3", "z", 256, 5),
+    ("m0", "y", 128, 1), ("m2", "z", 384, 1),
+    ("u0", "y", 256, 4), ("u1", "y", 128, 4), ("u2", "z", 640, 4),
+    ("d0", "y", 256, 5), ("d1", "y", 256, 5), ("d2", "z", 512, 5),
 )
-NOT_BEFORE = {4: 0.0, 5: 0.0}
-PRIORITY = {}
+HOPS = {
+    "m": {"y": (1.23, 2.17), "yz": (0.63, 0.88, 2.17, 0.68),
+     "z": (1.89, 0.6, 1.2, 0.71), "zy": (0.96, 1.71, 1.24, 0.91, 2.1)},
+    "u": {"y": (2.25, 1.09), "yz": (4.41, 4.71, 2.85, 4.22),
+     "z": (5.36, 1.97, 2.56, 5.09), "zy": (3.67, 2.93, 2.85, 3.49, 2.72)},
+    "d": {"y": (3.17, 2.62), "yz": (1.4, 5.34, 5.8, 2.75),
+     "z": (1.15, 2.53, 1.97, 4.54), "zy": (2.22, 4.61, 1.89, 4.39, 5.9)},
+}
 
 
 class Op:
@@ -56,10 +63,9 @@
         for at, op in enumerate(left):
             if any(d not in done for d in op.deps):
                 continue
-            ready = max([done[d] for d in op.deps], default=NOT_BEFORE.get(op.prio, 0.0))
-            ready = max(ready, NOT_BEFORE.get(op.prio, 0.0))
+            ready = max([done[d] for d in op.deps], default=0.0)
             if op.link is not None:
-                ready = max(ready, link_free.get(op.link, 0.0) - (BACKLOG if op.prio >= 3 else 3 * BACKLOG))
+                ready = max(ready, link_free.get(op.link, 0.0) - (BACKLOG if op.prio >= 3 else 1.48 * BACKLOG))
             key = (max(ready, now), op.prio, at)
             if best is None or key < best[0]:
                 best = (key, op)
@@ -172,67 +178,67 @@
     def y_first(tag, w, c0, n, deps, prio):
         size = ROWS * n * 2
         part_of = lambda zs, rows: (lambda: w.at[zs, rows, pl.ds(c0, n)])
-        sent_y = (f"{tag}.Y", part_of(0, pl.ds(0, 3 * ROWS)))
-        sent_z = (f"{tag}.Z", part_of(pl.ds(0, 7), pl.ds(0, GROUP)))
-        second = (f"{tag}.Y2", part_of(0, pl.ds(0, ROWS)))
-        fourth = (f"{tag}.Z4", part_of(0, pl.ds(0, GROUP)))
+        sent_y = ((tag, "Y"), part_of(0, pl.ds(0, 3 * ROWS)))
+        sent_z = ((tag, "Z"), part_of(pl.ds(0, 7), pl.ds(0, GROUP)))
+        second = ((tag, "Y", 2), part_of(0, pl.ds(0, ROWS)))
+        fourth = ((tag, "Z", 4), part_of(0, pl.ds(0, GROUP)))
         for d in "+-":
             s = sign[d]
             b = block(w, 0, 0, c0, n)
-            send(f"{tag}.Y1{d}", "y" + d, deps, b, b, block(w, 0, -s, c0, n), size,
-                 PRIORITY.get(f"{tag[0]}yY1", prio), sent_y)
+            send((tag, "Y", 1, d), "y" + d, deps, b, b, block(w, 0, -s, c0, n), size,
+                 HOPS[tag[0]]["y"][0], sent_y)
         for d, half in (("+", 0), ("-", 1)):
             s = sign[d]
             b = block(w, 0, -s, c0, n, half)
-            send(f"{tag}.Y2{d}", "y" + d, [f"{tag}.Y1{d}"], b, b, block(w, 0, -2 * s, c0, n, half), size // 2,
-                 PRIORITY.get(f"{tag[0]}yY2", prio), sent_y, second)
-        group = [f"{tag}.Y{h}{d}" for h in (1, 2) for d in "+-"]
+            send((tag, "Y", 2, d), "y" + d, [(tag, "Y", 1, d)], b, b, block(w, 0, -2 * s, c0, n, half), size // 2,
+                 HOPS[tag[0]]["y"][1], sent_y, second)
+        group = [(tag, "Y", h, d) for h in (1, 2) for d in "+-"]
         ready[tag[0], 0] = ready.get((tag[0], 0), []) + group
         for d, half in (("+", 0), ("-", 1)):
             s = sign[d]
             for h in (1, 2, 3, 4):
                 part = half if h == 4 else None
                 b = slab(w, -s * (h - 1), c0, n, part)
-                before = deps + group if h == 1 else [f"{tag}.Z{h - 1}{d}"]
-                send(f"{tag}.Z{h}{d}", "z" + d, before, b, b, slab(w, -s * h, c0, n, part),
-                     NY * size // (1 if part is None else 2), PRIORITY.get(f"{tag[0]}yZ{h}", prio),
+                before = deps + group if h == 1 else [(tag, "Z", h - 1, d)]
+                send((tag, "Z", h, d), "z" + d, before, b, b, slab(w, -s * h, c0, n, part),
+                     NY * size // (1 if part is None else 2), HOPS[tag[0]]["yz"][h - 1],
                      sent_z, fourth if h == 4 else None)
                 dist = 4 if h == 4 else -s * h
-                ready[tag[0], dist] = ready.get((tag[0], dist), []) + [f"{tag}.Z{h}{d}"]
+                ready[tag[0], dist] = ready.get((tag[0], dist), []) + [(tag, "Z", h, d)]
 
     def z_first(tag, w, c0, n, deps, prio):
         size = ROWS * n * 2
         part_of = lambda zs, rows: (lambda: w.at[zs, rows, pl.ds(c0, n)])
         sent_z = part_of(0, pl.ds(0, 7 * ROWS // 2))
-        sent_y = (f"{tag}.Y", part_of(pl.ds(0, 6), pl.ds(0, GROUP)))
-        fourth = (f"{tag}.Z4", part_of(0, pl.ds(0, ROWS)))
+        sent_y = ((tag, "Y"), part_of(pl.ds(0, 6), pl.ds(0, GROUP)))
+        fourth = ((tag, "Z", 4), part_of(0, pl.ds(0, ROWS)))
         for d, half in (("+", 0), ("-", 1)):
             s = sign[d]
             for h in (1, 2, 3, 4):
                 part = half if h == 4 else None
                 b = block(w, -s * (h - 1), 0, c0, n, part)
-                before = deps if h == 1 else [f"{tag}.Z{h - 1}{d}"]
-                send(f"{tag}.Z{h}{d}", "z" + d, before, b, b, block(w, -s * h, 0, c0, n, part),
-                     size // (1 if part is None else 2), PRIORITY.get(f"{tag[0]}zZ{h}", prio),
-                     (f"{tag}.Z{d}", sent_z), fourth if h == 4 else None)
+                before = deps if h == 1 else [(tag, "Z", h - 1, d)]
+                send((tag, "Z", h, d), "z" + d, before, b, b, block(w, -s * h, 0, c0, n, part),
+                     size // (1 if part is None else 2), HOPS[tag[0]]["z"][h - 1],
+                     ((tag, "Z", d), sent_z), fourth if h == 4 else None)
         for at, dist in enumerate(ARRIVAL):
-            here = {0: deps, 4: [f"{tag}.Z4+", f"{tag}.Z4-"]}.get(
-                dist, [f"{tag}.Z{abs(dist)}{'-' if dist > 0 else '+'}"])
+            here = {0: deps, 4: [(tag, "Z", 4, "+"), (tag, "Z", 4, "-")]}.get(
+                dist, [(tag, "Z", abs(dist), NEAR[dist > 0])])
             second = {
-                "m": (f"{tag}.Y2.{at}", part_of(0, pl.ds(0, ROWS))),
-                "u": (f"{tag}.Y2", part_of(pl.ds(0, 2), pl.ds(0, GROUP))),
-                "d": (f"{tag}.Y2.{at // 2}", part_of(0, pl.ds(0, 2 * ROWS))),
+                "m": ((tag, "Y", 2, at), part_of(0, pl.ds(0, ROWS))),
+                "u": ((tag, "Y", 2), part_of(pl.ds(0, 2), pl.ds(0, GROUP))),
+                "d": ((tag, "Y", 2, at // 2), part_of(0, pl.ds(0, 2 * ROWS))),
             }[tag[0]]
             for d, half in (("+", 0), ("-", 1)):
                 s = sign[d]
                 b = block(w, dist, 0, c0, n)
-                send(f"{tag}.Y1{d}{dist}", "y" + d, here, b, b, block(w, dist, -s, c0, n), size,
-                     PRIORITY.get(f"{tag[0]}zY{abs(dist)}", prio), sent_y)
+                send((tag, "Y", 1, d, dist), "y" + d, here, b, b, block(w, dist, -s, c0, n), size,
+                     HOPS[tag[0]]["zy"][abs(dist)], sent_y)
                 b = block(w, dist, -s, c0, n, half)
-                send(f"{tag}.Y2{d}{dist}", "y" + d, [f"{tag}.Y1{d}{dist}"], b, b,
+                send((tag, "Y", 2, d, dist), "y" + d, [(tag, "Y", 1, d, dist)], b, b,
                      block(w, dist, -2 * s, c0, n, half), size // 2,
-                     PRIORITY.get(f"{tag[0]}zY{abs(dist)}", prio), sent_y, second)
-            names = here + [f"{tag}.Y{h}{d}{dist}" for h in (1, 2) for d in "+-"]
+                     HOPS[tag[0]]["zy"][abs(dist)], sent_y, second)
+            names = here + [(tag, "Y", h, d, dist) for h in (1, 2) for d in "+-"]
             ready[tag[0], dist] = ready.get((tag[0], dist), []) + names
 
     seen = []
@@ -272,8 +278,8 @@
     compute_after = ["load.t"] + mixer_loads
     for dist in ARRIVAL:
         compute_after = compute_after + ready["m", dist]
-        compute(f"project{dist}", compute_after, project(dist == 0, [dist]), 0, 0.35)
-        compute_after = [f"project{dist}"]
+        compute(("project", dist), compute_after, project(dist == 0, [dist]), 0, 0.35)
+        compute_after = [("project", dist)]
     compute("convolve", compute_after, convolve, 0, 0.7)
 
     nt = (((1,), (1,)), ((), ()))
@@ -294,33 +300,33 @@
         return pl.ds(pl.multiple_of(p * PART + core * CORE_ROWS + mod(x + dx, NX) * OWN, OWN), OWN)
 
     def sum_chunk(phase, p, k, groups, residual, prio):
-        t = f"s{phase}{p}.{k}"
+        t = ("s", phase, p, k)
         d, e = ("+", "-") if k % 2 == 0 else ("-", "+")
         s = sign[d]
-        send(f"{t}.pair", "c", [f"{t}.product"], lambda: pp.at[phase, p, k, core_rows(1 - c), :],
+        send((t, "pair"), "c", [(t, "product")], lambda: pp.at[phase, p, k, core_rows(1 - c), :],
              lambda: dr.at[phase, p, k], lambda: dr.at[phase, p, k], CORE_ROWS * CHUNK * 2, prio,
-             (f"s{phase}{p}.pair", lambda: dr.at[phase, p]))
+             (("s", phase, p, "pair"), lambda: dr.at[phase, p]))
 
         def add_pair():
             so[phase, p, k] = (
                 pp[phase, p, k, core_rows(c), :].astype(f32) + dr[phase, p, k].astype(f32)).astype(bf16)
 
-        compute(f"{t}.add", [f"{t}.product", f"{t}.pair"], add_pair, prio, 0.06)
+        compute((t, "add"), [(t, "product"), (t, "pair")], add_pair, prio, 0.06)
         size = OWN * CHUNK * 2
         at = lambda dx: (lambda: so.at[phase, p, k, rows_of(dx), :])
         slot = lambda ref: (lambda: ref.at[phase, p, k])
-        sent = (f"s{phase}{p}.x", lambda: so.at[phase, p, pl.ds(0, CHUNKS - 1)])
-        last = (f"{t}.last", lambda: so.at[phase, p, k, pl.ds(0, 2 * OWN), :])
-        send(f"{t}.relay", "x" + d, [f"{t}.add"], at(2), slot(rl), slot(rl), size, prio, sent)
-        send(f"{t}.direct", "x" + e, [f"{t}.add"], at(-s), slot(fd), slot(fd), size, prio + 0.5,
+        sent = (("s", phase, p, "x"), lambda: so.at[phase, p, pl.ds(0, CHUNKS - 1)])
+        last = ((t, "last"), lambda: so.at[phase, p, k, pl.ds(0, 2 * OWN), :])
+        send((t, "relay"), "x" + d, [(t, "add")], at(2), slot(rl), slot(rl), size, prio, sent)
+        send((t, "direct"), "x" + e, [(t, "add")], at(-s), slot(fd), slot(fd), size, prio + 0.5,
              sent, last)
 
         def add_relay():
             so[phase, p, k, rows_of(s), :] = (
                 so[phase, p, k, rows_of(s), :].astype(f32) + rl[phase, p, k].astype(f32)).astype(bf16)
 
-        compute(f"{t}.radd", [f"{t}.add", f"{t}.relay"], add_relay, prio, 0.03)
-        send(f"{t}.final", "x" + d, [f"{t}.radd"], at(s), slot(fr), slot(fr), size, prio, sent, last)
+        compute((t, "radd"), [(t, "add"), (t, "relay")], add_relay, prio, 0.03)
+        send((t, "final"), "x" + d, [(t, "radd")], at(s), slot(fr), slot(fr), size, prio, sent, last)
 
         def finish():
             total = so[phase, p, k, rows_of(0), :].astype(f32) + fr[phase, p, k].astype(f32)
@@ -330,7 +336,7 @@
                 v[p, :, columns] = (residual_scale * residual[seq_rows(p), columns].astype(f32)
                                     + total[:, at * GROUP:(at + 1) * GROUP])
 
-        compute(f"{t}.finish", [f"{t}.add", f"{t}.final", f"{t}.direct"], finish, prio, 0.04)
+        compute((t, "finish"), [(t, "add"), (t, "final"), (t, "direct")], finish, prio, 0.04)
 
     def norm(phase, p, gain, shift, dest, prio):
         def emit():
@@ -341,7 +347,7 @@
             scaled = centered * lax.rsqrt(variance + norm_epsilon)
             dest[seq_rows(p), :] = (scaled * gain[...] + shift[...]).astype(bf16)
 
-        compute(f"norm{phase}{p}", [f"s{phase}{p}.{k}.finish" for k in range(CHUNKS)], emit, prio, 0.25)
+        compute(("norm", phase, p), [(("s", phase, p, k), "finish") for k in range(CHUNKS)], emit, prio, 0.25)
 
     HALF = WIDTH // 2
 
@@ -355,30 +361,30 @@
         def at(*where):
             return lambda: place(p, *where)(ref)
 
-        t, size, landed = f"g{phase}{p}", OWN * HALF * 2, []
-        start = [f"norm{phase}{p}"]
+        t, size, landed = ("g", phase, p), OWN * HALF * 2, []
+        start = [("norm", phase, p)]
         first_rows = lambda rows: (lambda: ref.at[pl.ds(0, rows), :])
-        sent_x, sent_c = (f"{t}.x", first_rows(3 * OWN)), (f"{t}.c", first_rows(4 * OWN))
+        sent_x, sent_c = ((t, "x"), first_rows(3 * OWN)), ((t, "c"), first_rows(4 * OWN))
         if phase == 0:
-            pairs = [(f"{t}.P", first_rows(4 * OWN))] * 4
+            pairs = [((t, "P"), first_rows(4 * OWN))] * 4
         else:
-            pairs = [(f"{t}.P{i}", first_rows(rows)) for i, rows in enumerate((OWN, OWN, OWN, OWN))]
+            pairs = [((t, "P", i), first_rows(rows)) for i, rows in enumerate((OWN, OWN, OWN, OWN))]
         for d, first_half in (("+", 0), ("-", 1)):
             for h in (first_half, 1 - first_half):
-                send(f"{t}.A{d}{h}", "x" + d, start, at(0, h), at(0, h), at(-sign[d], h), size, prio, sent_x)
-                landed.append((f"{t}.A{d}{h}", (-sign[d], h)))
-        send(f"{t}.P", "c", start, at(0, None), at(0, None), at(0, None, True), 2 * size, prio, sent_c, pairs[0])
-        landed.append((f"{t}.P", (0, None, True)))
+                send((t, "A", d, h), "x" + d, start, at(0, h), at(0, h), at(-sign[d], h), size, prio, sent_x)
+                landed.append(((t, "A", d, h), (-sign[d], h)))
+        send((t, "P"), "c", start, at(0, None), at(0, None), at(0, None, True), 2 * size, prio, sent_c, pairs[0])
+        landed.append(((t, "P"), (0, None, True)))
         for d, h in (("+", 0), ("-", 1)):
             b = at(-sign[d], h)
-            send(f"{t}.B{d}", "x" + d, [f"{t}.A{d}{h}"], b, b, at(2, h), size, prio, sent_x)
-            landed.append((f"{t}.B{d}", (2, h)))
+            send((t, "B", d), "x" + d, [(t, "A", d, h)], b, b, at(2, h), size, prio, sent_x)
+            landed.append(((t, "B", d), (2, h)))
         for i, (name, dx, h) in enumerate((
-                (f"{t}.A+0", -1, 0), (f"{t}.A-1", 1, 1), (f"{t}.A+1", -1, 1),
-                (f"{t}.A-0", 1, 0), (f"{t}.B+", 2, 0), (f"{t}.B-", 2, 1))):
-            send(f"{name}.P", "c", [name], at(dx, h), at(dx, h), at(dx, h, True), size, prio,
+                ((t, "A", "+", 0), -1, 0), ((t, "A", "-", 1), 1, 1), ((t, "A", "+", 1), -1, 1),
+                ((t, "A", "-", 0), 1, 0), ((t, "B", "+"), 2, 0), ((t, "B", "-"), 2, 1))):
+            send((name, "P"), "c", [name], at(dx, h), at(dx, h), at(dx, h, True), size, prio,
                  sent_c, pairs[1 + i // 2])
-            landed.append((f"{name}.P", (dx, h, True)))
+            landed.append(((name, "P"), (dx, h, True)))
         return landed
 
     def hidden(p, n):
@@ -392,20 +398,20 @@
     for p in range(PARTS):
         for k in range(CHUNKS):
             pair = (2 * k, 2 * k + 1)
-            compute(f"s0{p}.{k}.product", ["convolve"],
+            compute((("s", 0, p, k), "product"), ["convolve"],
                     functools.partial(product, 0, p, k, conv, [lambda g=g: wm[g, :, 384:512] for g in pair]),
                     0 + p, 0.25)
             sum_chunk(0, p, k, [lambda g=g: g for g in pair], tok, 0 + p)
         norm(0, p, mgain, mshift, first, 0 + p)
         landed = gather(0, p, first, 0 + p)
         for n in range(2):
-            compute(f"hidden{p}{n}", [f"norm0{p}"] + [name for name, _ in landed] + up_ready,
+            compute(("hidden", p, n), [("norm", 0, p)] + [name for name, _ in landed] + up_ready,
                     functools.partial(hidden, p, n), 2 + p, 0.75)
         for k in range(CHUNKS):
             dists = ARRIVAL[2 * k:2 * k + 2]
             groups = [lambda dist=dist: mod(zl + dist, NZ) for dist in dists]
             arrived = [name for dist in dists for name in ready["d", dist]]
-            compute(f"s1{p}.{k}.product", [f"hidden{p}{n}" for n in range(2)] + ["load.d"] + arrived,
+            compute((("s", 1, p, k), "product"), [("hidden", p, n) for n in range(2)] + ["load.d"] + arrived,
                     functools.partial(product, 1, p, k, hid, [lambda g=g: wd[g()] for g in groups]),
                     2 + p, 0.5)
             sum_chunk(1, p, k, groups, first, 2 + p)
@@ -445,7 +451,7 @@
         wait()
 
 
-N_SENDS, N_RECVS, N_LOADS = 43, 275, 7
+N_SENDS, N_RECVS, N_LOADS = 35, 214, 7
 
 
 def local(tokens, gate_outer, gate_inner, conv_input, mixer_output, conv_taps, mixer_gain,

time: 107 us -> 101 us (0.944)
  Pallas kernels: 105 us -> 99.6 us
    pallas_call x1, Pallas kernels: 105 us -> 99.6 us  [local(): pl.pallas_call(layer_kernel, out_shape=pltpu.VMEM((SEQ, WIDTH), bf16), in...]
where the time goes in v4:
time: 101 us
  Pallas kernels  99.6 us (99%)
  local copies, waits for them, and re-layouts  1.32 us (1%)
    pallas_call x1, Pallas kernels, local(): pl.pallas_call(layer_kernel, out_shape=pltpu.VMEM((SEQ, WIDTH), bf16), in...  99.6 us

profile of v4, /device:TPU:1, one launch (start us, length us, event | category | flops | bytes accessed | tf_op | source)
XLA Modules:
  0.0 101.0 jit_solution(16729158546500524250)
XLA Ops:
  0.0 99.6 %shard_map.118 = bf16[512,2048]{1,0:T(8,128)(2,1)S(1)} custom-call(bf16[512,2048]{1,0:T(8,128)(2,1)} %tok_hbm.1, bf16[64,128]{1,0:T(8,128)(2,1)} %go_hbm.1, bf16[64,128]{1,0:T(8,128)(2,1)} %gi_hbm.1, bf16[64,128]{1,0:T(8,128)(2,1)} %ci_hbm.1, bf16[64,128]{1,0:T(8,128)(2,1)} %mo_hbm.1, bf16[64,1024]{1,0:T(8,128)(2,1)} %up_hbm.1, bf16[64,1024]{1,0:T(8,128)(2,1)} %dn_hbm.1, ...), custom_call_target="tpu_custom_call" | custom-call | tf_op jit(solution)/shard_map/pallas_call | solution.py:461
  99.6 1.3 %copy.14 = bf16[512,2048]{1,0:T(8,128)(2,1)} copy(bf16[512,2048]{1,0:T(8,128)(2,1)S(1)} %shard_map.118) | data formatting | bytes 4194304

commit v5 on v4

--- a/solution.py
+++ b/solution.py
@@ -20,10 +20,13 @@
 CHUNKS, CHUNK = 4, 512
 NEAR = ("+", "-")
 ARRIVAL = (0, 1, -1, 2, -2, 3, -3, 4)
+LATE = ((0, 1), (-1, 2), (-2, 3), (-3,), (4,))
+DIRECT = (False, False, False, False, True)
 
 LINK_RATE, LINK_LAT = 46.6e3, 1.9
 PAIR_RATE, PAIR_LAT = 500e3, 1.1
 BACKLOG = 1.08
+PATHS = {"c": (PAIR_RATE, PAIR_LAT), "x2": (LINK_RATE, 2.6)}
 
 
 PIECES = (
@@ -75,7 +78,7 @@
         if op.link is None:
             done[op.name] = now + op.latency
         else:
-            rate, lat = (PAIR_RATE, PAIR_LAT) if op.link == "c" else (LINK_RATE, LINK_LAT)
+            rate, lat = PATHS.get(op.link, (LINK_RATE, LINK_LAT))
             begin = max(now, link_free.get(op.link, 0.0))
             link_free[op.link] = begin + op.nbytes / rate
             done[op.name] = link_free[op.link] + lat
@@ -87,7 +90,7 @@
     tok_hbm, go_hbm, gi_hbm, ci_hbm, mo_hbm, up_hbm, dn_hbm, taps, mgain, mshift, cgain, cshift,
     res,
     tok, wm, wu, wd, proj, prod, conv, pp, so, dr, rl, fr, fd, v, first, hid,
-    send_sems, recv_sems, load_sems,
+    pp1, dr1, so1, in1, cs1, val, stats, send_sems, recv_sems, load_sems,
     report=None,
 ):
     f32, bf16 = jnp.float32, jnp.bfloat16
@@ -109,7 +112,7 @@
 
     peer = {
         "z+": device(dz=1), "z-": device(dz=-1), "y+": device(dy=1), "y-": device(dy=-1),
-        "x+": device(dx=1), "x-": device(dx=-1), "c": device(dc=1),
+        "x+": device(dx=1), "x-": device(dx=-1), "x2": device(dx=2), "c": device(dc=1),
     }
     sign = {"+": 1, "-": -1}
 
@@ -221,13 +224,14 @@
                 send((tag, "Z", h, d), "z" + d, before, b, b, block(w, -s * h, 0, c0, n, part),
                      size // (1 if part is None else 2), HOPS[tag[0]]["z"][h - 1],
                      ((tag, "Z", d), sent_z), fourth if h == 4 else None)
+        late = {dist: j for j, dists in enumerate(LATE) for dist in dists}
         for at, dist in enumerate(ARRIVAL):
             here = {0: deps, 4: [(tag, "Z", 4, "+"), (tag, "Z", 4, "-")]}.get(
                 dist, [(tag, "Z", abs(dist), NEAR[dist > 0])])
             second = {
                 "m": ((tag, "Y", 2, at), part_of(0, pl.ds(0, ROWS))),
                 "u": ((tag, "Y", 2), part_of(pl.ds(0, 2), pl.ds(0, GROUP))),
-                "d": ((tag, "Y", 2, at // 2), part_of(0, pl.ds(0, 2 * ROWS))),
+                "d": ((tag, "Y", 2, late[dist]), part_of(0, pl.ds(0, ROWS * len(LATE[late[dist]])))),
             }[tag[0]]
             for d, half in (("+", 0), ("-", 1)):
                 s = sign[d]
@@ -407,16 +411,140 @@
         for n in range(2):
             compute(("hidden", p, n), [("norm", 0, p)] + [name for name, _ in landed] + up_ready,
                     functools.partial(hidden, p, n), 2 + p, 0.75)
-        for k in range(CHUNKS):
-            dists = ARRIVAL[2 * k:2 * k + 2]
-            groups = [lambda dist=dist: mod(zl + dist, NZ) for dist in dists]
-            arrived = [name for dist in dists for name in ready["d", dist]]
-            compute((("s", 1, p, k), "product"), [("hidden", p, n) for n in range(2)] + ["load.d"] + arrived,
-                    functools.partial(product, 1, p, k, hid, [lambda g=g: wd[g()] for g in groups]),
-                    2 + p, 0.5)
-            sum_chunk(1, p, k, groups, first, 2 + p)
-        norm(1, p, cgain, cshift, res, 2 + p)
-        gather(1, p, res, 2 + p)
+
+    own_block, half_of = ROWS, SEQ // 2
+
+    def late_rows(dx=0, core=None, rows=own_block, off=0):
+        core = c if core is None else core
+        start = core * half_of + mod(x + dx, NX) * own_block + off
+        return pl.ds(pl.multiple_of(start, own_block // 2), rows)
+
+    def late_half(core):
+        return pl.ds(pl.multiple_of(core * half_of, half_of), half_of)
+
+    def in_half(dx):
+        return pl.ds(pl.multiple_of(mod(x + dx, NX) * own_block, own_block), own_block)
+
+    def late_chunk(j, dists, direct, prio):
+        t, width = ("late", j), GROUP * len(dists)
+        wide = pl.ds(0, width)
+        groups = [mod(zl + dist, NZ) for dist in dists]
+        columns = [pl.ds(pl.multiple_of(g * GROUP, GROUP), GROUP) for g in groups]
+        arrived = [name for dist in dists for name in ready["d", dist]]
+
+        def multiply():
+            for at, g in enumerate(groups):
+                for r in range(2):
+                    rows = pl.ds(r * half_of, half_of)
+                    pp1[j, rows, at * GROUP:(at + 1) * GROUP] = lax.dot_general(
+                        hid[rows, :], wd[g], nt, preferred_element_type=f32).astype(bf16)
+
+        compute((t, "product"), [("hidden", p, n) for p in range(PARTS) for n in range(2)] + ["load.d"] + arrived,
+                multiply, prio, 0.5 * len(dists))
+        sent_x = ((t, "x"), lambda: cs1.at[j, pl.ds(0, 6 * own_block), wide])
+        sent_c = ((t, "c"), lambda: cs1.at[j, :, wide])
+        size = own_block * width * 2
+        send((t, "pair"), "c", [(t, "product")], lambda: pp1.at[j, late_half(1 - c), wide],
+             lambda: dr1.at[j, :, wide], lambda: dr1.at[j, :, wide], NX * size, prio, sent_c)
+
+        def add_pair():
+            so1[j, :, wide] = (
+                pp1[j, late_half(c), wide].astype(f32) + dr1[j, :, wide].astype(f32)).astype(bf16)
+
+        compute((t, "add"), [(t, "pair")], add_pair, prio, 0.1)
+        at = lambda dx: (lambda: so1.at[j, in_half(dx), wide])
+        slot = lambda i: (lambda: in1.at[j, i, :, wide])
+        d, e = ("+", "-") if j % 2 == 0 else ("-", "+")
+        s = sign[d]
+        if direct:
+            last = ((t, "last"), lambda: so1.at[j, pl.ds(0, 3 * own_block), wide])
+            send((t, "far"), "x2", [(t, "add")], at(2), slot(0), slot(0), size, prio, sent_x, last)
+            send((t, "plus"), "x+", [(t, "add")], at(1), slot(1), slot(1), size, prio, sent_x, last)
+            send((t, "minus"), "x-", [(t, "add")], at(-1), slot(2), slot(2), size, prio, sent_x, last)
+            terms, from_others = (0, 1, 2), [(t, "far"), (t, "plus"), (t, "minus")]
+        else:
+            last = ((t, "last"), lambda: so1.at[j, pl.ds(0, 2 * own_block), wide])
+            send((t, "relay"), "x" + d, [(t, "add")], at(2), slot(0), slot(0), size, prio, sent_x)
+            send((t, "direct"), "x" + e, [(t, "add")], at(-s), slot(2), slot(2), size, prio + 0.5, sent_x, last)
+
+            def add_relay():
+                so1[j, in_half(s), wide] = (
+                    so1[j, in_half(s), wide].astype(f32) + in1[j, 0, :, wide].astype(f32)).astype(bf16)
+
+            compute((t, "radd"), [(t, "relay")], add_relay, prio, 0.05)
+            send((t, "final"), "x" + d, [(t, "radd")], at(s), slot(1), slot(1), size, prio, sent_x, last)
+            terms, from_others = (1, 2), [(t, "final"), (t, "direct")]
+
+        def finish():
+            total = so1[j, in_half(0), wide].astype(f32)
+            for i in terms:
+                total = total + in1[j, i, :, wide].astype(f32)
+            cs1[j, late_rows(), wide] = total.astype(bf16)
+
+        compute((t, "finish"), from_others, finish, prio, 0.06)
+
+        def there(*where, **more):
+            return lambda: cs1.at[j, late_rows(*where, **more), wide]
+
+        begin = [(t, "finish")]
+        paired = ((t, "P"), lambda: cs1.at[j, pl.ds(0, half_of), wide])
+        other = 1 - c
+        send((t, "A", "+"), "x+", begin, there(0), there(0), there(-1), size, prio, sent_x)
+        send((t, "A", "-"), "x-", begin, there(0), there(0), there(1), size, prio, sent_x)
+        if direct:
+            send((t, "A", "x2"), "x2", begin, there(0), there(0), there(2), size, prio, sent_x)
+            far = [(t, "A", "x2")]
+        else:
+            both = ((t, "B"), there(2))
+            for d, off in (("+", 0), ("-", own_block // 2)):
+                piece = dict(rows=own_block // 2, off=off)
+                b = there(-sign[d], **piece)
+                send((t, "B", d), "x" + d, [(t, "A", d)], b, b, there(2, **piece), size // 2, prio, sent_x, both)
+            far = [(t, "B", "+"), (t, "B", "-")]
+        for dx, after in ((0, begin), (-1, [(t, "A", "+")]), (1, [(t, "A", "-")]), (2, far)):
+            send((t, "P", dx), "c", after, there(dx), there(dx), there(dx, other), size, prio, sent_c, paired)
+
+        def count():
+            def step(i, _):
+                rows = pl.ds(pl.multiple_of(i * 64, 64), 64)
+                for at, cols in enumerate(columns):
+                    value = (residual_scale * first[rows, cols].astype(f32)
+                             + cs1[j, rows, at * GROUP:(at + 1) * GROUP].astype(f32))
+                    val[rows, cols] = value
+                    if j == 0 and at == 0:
+                        stats[0, rows, :] = jnp.mean(value, -1, keepdims=True)
+                    value = value - stats[0, rows, :]
+                    one = jnp.sum(value, -1, keepdims=True)
+                    two = jnp.sum(value * value, -1, keepdims=True)
+                    if j == 0 and at == 0:
+                        stats[1, rows, :], stats[2, rows, :] = one, two
+                    else:
+                        stats[1, rows, :] += one
+                        stats[2, rows, :] += two
+                return 0
+
+            lax.fori_loop(0, SEQ // 64, step, 0)
+
+        compute((t, "count"), begin + far + [(t, "P", dx) for dx in (0, -1, 1, 2)]
+                + ([("late", j - 1, "count")] if j else []), count, prio, 0.3 * len(dists))
+        ops[-1].name = ("late", j, "count")
+
+    for j, dists in enumerate(LATE):
+        late_chunk(j, dists, DIRECT[j], 2 + 0.1 * j)
+
+    def finish_norm():
+        def step(i, _):
+            rows = pl.ds(pl.multiple_of(i * 64, 64), 64)
+            off = stats[1, rows, :] * (1.0 / WIDTH)
+            variance = jnp.maximum(stats[2, rows, :] * (1.0 / WIDTH) - off * off, 0.0)
+            scale = lax.rsqrt(variance + norm_epsilon)
+            centered = val[rows, :] - (stats[0, rows, :] + off)
+            res[rows, :] = (centered * scale * cgain[...] + cshift[...]).astype(bf16)
+            return 0
+
+        lax.fori_loop(0, SEQ // 64, step, 0)
+
+    compute("finish_norm", [("late", j, "count") for j in range(len(LATE))], finish_norm, 0, 1.2)
 
     order, done = plan(ops)
     if report is not None:
@@ -451,7 +579,7 @@
         wait()
 
 
-N_SENDS, N_RECVS, N_LOADS = 35, 214, 7
+N_SENDS, N_RECVS, N_LOADS = 37, 205, 7
 
 
 def local(tokens, gate_outer, gate_inner, conv_input, mixer_output, conv_taps, mixer_gain,
@@ -471,21 +599,28 @@
             pltpu.VMEM((SEQ, 384), f32),
             pltpu.VMEM((SEQ + 8, 128), f32),
             pltpu.VMEM((SEQ, 128), bf16),
-            pltpu.VMEM((2, PARTS, CHUNKS, PART, CHUNK), bf16),
-            pltpu.VMEM((2, PARTS, CHUNKS, CORE_ROWS, CHUNK), bf16),
-            pltpu.VMEM((2, PARTS, CHUNKS, CORE_ROWS, CHUNK), bf16),
-            pltpu.VMEM((2, PARTS, CHUNKS, OWN, CHUNK), bf16),
-            pltpu.VMEM((2, PARTS, CHUNKS, OWN, CHUNK), bf16),
-            pltpu.VMEM((2, PARTS, CHUNKS, OWN, CHUNK), bf16),
+            pltpu.VMEM((1, PARTS, CHUNKS, PART, CHUNK), bf16),
+            pltpu.VMEM((1, PARTS, CHUNKS, CORE_ROWS, CHUNK), bf16),
+            pltpu.VMEM((1, PARTS, CHUNKS, CORE_ROWS, CHUNK), bf16),
+            pltpu.VMEM((1, PARTS, CHUNKS, OWN, CHUNK), bf16),
+            pltpu.VMEM((1, PARTS, CHUNKS, OWN, CHUNK), bf16),
+            pltpu.VMEM((1, PARTS, CHUNKS, OWN, CHUNK), bf16),
             pltpu.VMEM((PARTS, OWN, WIDTH), f32),
             pltpu.VMEM((SEQ, WIDTH), bf16),
             pltpu.VMEM((SEQ, 1024), bf16),
+            pltpu.VMEM((len(LATE), SEQ, CHUNK), bf16),
+            pltpu.VMEM((len(LATE), SEQ // 2, CHUNK), bf16),
+            pltpu.VMEM((len(LATE), SEQ // 2, CHUNK), bf16),
+            pltpu.VMEM((len(LATE), 3, ROWS, CHUNK), bf16),
+            pltpu.VMEM((len(LATE), SEQ, CHUNK), bf16),
+            pltpu.VMEM((SEQ, WIDTH), f32),
+            pltpu.VMEM((3, SEQ, 1), f32),
             pltpu.SemaphoreType.DMA((N_SENDS,)),
             pltpu.SemaphoreType.DMA((N_RECVS,)),
             pltpu.SemaphoreType.DMA((N_LOADS,)),
         ],
         compiler_params=pltpu.CompilerParams(
-            collective_id=0, has_side_effects=True, vmem_limit_bytes=60 * 2**20),
+            collective_id=0, has_side_effects=True, vmem_limit_bytes=56 * 2**20),
     )(tokens, gate_outer, gate_inner, conv_input, mixer_output, up_weight, down_weight, conv_taps,
       mixer_gain.reshape(1, -1), mixer_shift.reshape(1, -1), channel_gain.reshape(1, -1),
       channel_shift.reshape(1, -1))

time: 101 us -> 109 us (1.079)
  Pallas kernels: 99.6 us -> 108 us
    pallas_call x1, Pallas kernels: 99.6 us -> 108 us  [local(): pl.pallas_call(layer_kernel, out_shape=pltpu.VMEM((SEQ, WIDTH), bf16), in...]
where the time goes in v5:
time: 109 us
  Pallas kernels  108 us (99%)
  local copies, waits for them, and re-layouts  1.32 us (1%)
    pallas_call x1, Pallas kernels, local(): pl.pallas_call(layer_kernel, out_shape=pltpu.VMEM((SEQ, WIDTH), bf16), in...  108 us

profile of v5, /device:TPU:1, one launch (start us, length us, event | category | flops | bytes accessed | tf_op | source)
XLA Modules:
  0.0 108.9 jit_solution(11699055405155681365)
XLA Ops:
  0.0 107.5 %shard_map.118 = bf16[512,2048]{1,0:T(8,128)(2,1)S(1)} custom-call(bf16[512,2048]{1,0:T(8,128)(2,1)} %tok_hbm.1, bf16[64,128]{1,0:T(8,128)(2,1)} %go_hbm.1, bf16[64,128]{1,0:T(8,128)(2,1)} %gi_hbm.1, bf16[64,128]{1,0:T(8,128)(2,1)} %ci_hbm.1, bf16[64,128]{1,0:T(8,128)(2,1)} %mo_hbm.1, bf16[64,1024]{1,0:T(8,128)(2,1)} %up_hbm.1, bf16[64,1024]{1,0:T(8,128)(2,1)} %dn_hbm.1, ...), custom_call_target="tpu_custom_call" | custom-call | tf_op jit(solution)/shard_map/pallas_call | solution.py:589
  107.5 1.3 %copy.14 = bf16[512,2048]{1,0:T(8,128)(2,1)} copy(bf16[512,2048]{1,0:T(8,128)(2,1)S(1)} %shard_map.118) | data formatting | bytes 4194304

commit v6 on v5

--- a/solution.py
+++ b/solution.py
@@ -21,34 +21,41 @@
 NEAR = ("+", "-")
 ARRIVAL = (0, 1, -1, 2, -2, 3, -3, 4)
 LATE = ((0, 1), (-1, 2), (-2, 3), (-3,), (4,))
-DIRECT = (False, False, False, False, True)
+DIRECT = (False, False, False, True, True)
 
 LINK_RATE, LINK_LAT = 46.6e3, 1.9
 PAIR_RATE, PAIR_LAT = 500e3, 1.1
-BACKLOG = 1.08
+BACKLOG = 2.39
 PATHS = {"c": (PAIR_RATE, PAIR_LAT), "x2": (LINK_RATE, 2.6)}
 
 
 PIECES = (
-    ("m0", "y", 128, 1), ("m2", "z", 384, 1),
-    ("u0", "y", 256, 4), ("u1", "y", 128, 4), ("u2", "z", 640, 4),
-    ("d0", "y", 256, 5), ("d1", "y", 256, 5), ("d2", "z", 512, 5),
+    ("m0", "y", 128, 1),
+    ("m2", "z", 384, 1),
+    ("u0", "y", 128, 4),
+    ("u1", "y", 256, 4),
+    ("u2", "z", 384, 4),
+    ("u3", "z", 256, 4),
+    ("d0", "y", 256, 5),
+    ("d1", "y", 256, 5),
+    ("d2", "z", 512, 5),
 )
 HOPS = {
-    "m": {"y": (1.23, 2.17), "yz": (0.63, 0.88, 2.17, 0.68),
-     "z": (1.89, 0.6, 1.2, 0.71), "zy": (0.96, 1.71, 1.24, 0.91, 2.1)},
-    "u": {"y": (2.25, 1.09), "yz": (4.41, 4.71, 2.85, 4.22),
-     "z": (5.36, 1.97, 2.56, 5.09), "zy": (3.67, 2.93, 2.85, 3.49, 2.72)},
-    "d": {"y": (3.17, 2.62), "yz": (1.4, 5.34, 5.8, 2.75),
-     "z": (1.15, 2.53, 1.97, 4.54), "zy": (2.22, 4.61, 1.89, 4.39, 5.9)},
+    "m": {"y": (2.13, 0.62), "yz": (5.5, 0.56, 5.79, 3.68),
+          "z": (1.2, 3.12, 3.32, 4.69), "zy": (4.31, 4.14, 4.44, 5.8, 5.47)},
+    "u": {"y": (4.44, 2.55), "yz": (6, 3.2, 6, 1.93),
+          "z": (0.3, 5.81, 6, 3.59), "zy": (0.72, 0.66, 0.77, 6, 1.06)},
+    "d": {"y": (4.84, 3.77), "yz": (2.16, 3.17, 1.76, 5.74),
+          "z": (0.3, 3.82, 4.28, 6), "zy": (3.88, 1.07, 5.66, 2.05, 2.8)},
 }
+EARLIEST = {"uz": 7.5, "dy": 8.8, "dz": 15.2}
 
 
 class Op:
     def __init__(self, name, deps, emit, prio, dur=0.0, link=None, nbytes=0, wait=None, latency=0.0):
         self.name, self.deps, self.emit, self.prio = name, deps, emit, prio
         self.dur, self.link, self.nbytes, self.wait = dur, link, nbytes, wait
-        self.latency, self.group = latency, None
+        self.latency, self.group, self.earliest = latency, None, 0.0
 
 
 def plan(ops):
@@ -66,9 +73,9 @@
         for at, op in enumerate(left):
             if any(d not in done for d in op.deps):
                 continue
-            ready = max([done[d] for d in op.deps], default=0.0)
+            ready = max([done[d] for d in op.deps] + [op.earliest])
             if op.link is not None:
-                ready = max(ready, link_free.get(op.link, 0.0) - (BACKLOG if op.prio >= 3 else 1.48 * BACKLOG))
+                ready = max(ready, link_free.get(op.link, 0.0) - (BACKLOG if op.prio >= 3 else 0.65 * BACKLOG))
             key = (max(ready, now), op.prio, at)
             if best is None or key < best[0]:
                 best = (key, op)
@@ -412,7 +419,7 @@
             compute(("hidden", p, n), [("norm", 0, p)] + [name for name, _ in landed] + up_ready,
                     functools.partial(hidden, p, n), 2 + p, 0.75)
 
-    own_block, half_of = ROWS, SEQ // 2
+    own_block, half_of = OWN, CORE_ROWS
 
     def late_rows(dx=0, core=None, rows=own_block, off=0):
         core = c if core is None else core
@@ -425,8 +432,8 @@
     def in_half(dx):
         return pl.ds(pl.multiple_of(mod(x + dx, NX) * own_block, own_block), own_block)
 
-    def late_chunk(j, dists, direct, prio):
-        t, width = ("late", j), GROUP * len(dists)
+    def late_chunk(p, j, dists, direct, prio):
+        t, width = ("late", p, j), GROUP * len(dists)
         wide = pl.ds(0, width)
         groups = [mod(zl + dist, NZ) for dist in dists]
         columns = [pl.ds(pl.multiple_of(g * GROUP, GROUP), GROUP) for g in groups]
@@ -434,60 +441,60 @@
 
         def multiply():
             for at, g in enumerate(groups):
-                for r in range(2):
-                    rows = pl.ds(r * half_of, half_of)
-                    pp1[j, rows, at * GROUP:(at + 1) * GROUP] = lax.dot_general(
-                        hid[rows, :], wd[g], nt, preferred_element_type=f32).astype(bf16)
-
-        compute((t, "product"), [("hidden", p, n) for p in range(PARTS) for n in range(2)] + ["load.d"] + arrived,
-                multiply, prio, 0.5 * len(dists))
-        sent_x = ((t, "x"), lambda: cs1.at[j, pl.ds(0, 6 * own_block), wide])
-        sent_c = ((t, "c"), lambda: cs1.at[j, :, wide])
+                for r in range(1, -1, -1) if len(groups) == 1 else (None,):
+                    size, start = (PART, 0) if r is None else (half_of, r * half_of)
+                    pp1[p, j, pl.ds(start, size), at * GROUP:(at + 1) * GROUP] = lax.dot_general(
+                        hid[pl.ds(p * PART + start, size), :], wd[g], nt, preferred_element_type=f32).astype(bf16)
+
+        compute((t, "product"), [("hidden", p, n) for n in range(2)] + ["load.d"] + arrived,
+                multiply, prio, 0.25 * len(dists))
+        sent_x = ((t, "x"), lambda: cs1.at[p, j, pl.ds(0, 6 * own_block), wide])
+        sent_c = ((t, "c"), lambda: cs1.at[p, j, :, wide])
         size = own_block * width * 2
-        send((t, "pair"), "c", [(t, "product")], lambda: pp1.at[j, late_half(1 - c), wide],
-             lambda: dr1.at[j, :, wide], lambda: dr1.at[j, :, wide], NX * size, prio, sent_c)
+        send((t, "pair"), "c", [(t, "product")], lambda: pp1.at[p, j, late_half(1 - c), wide],
+             lambda: dr1.at[p, j, :, wide], lambda: dr1.at[p, j, :, wide], NX * size, prio, sent_c)
 
         def add_pair():
-            so1[j, :, wide] = (
-                pp1[j, late_half(c), wide].astype(f32) + dr1[j, :, wide].astype(f32)).astype(bf16)
+            so1[p, j, :, wide] = (
+                pp1[p, j, late_half(c), wide].astype(f32) + dr1[p, j, :, wide].astype(f32)).astype(bf16)
 
         compute((t, "add"), [(t, "pair")], add_pair, prio, 0.1)
-        at = lambda dx: (lambda: so1.at[j, in_half(dx), wide])
-        slot = lambda i: (lambda: in1.at[j, i, :, wide])
+        at = lambda dx: (lambda: so1.at[p, j, in_half(dx), wide])
+        slot = lambda i: (lambda: in1.at[p, j, i, :, wide])
         d, e = ("+", "-") if j % 2 == 0 else ("-", "+")
         s = sign[d]
         if direct:
-            last = ((t, "last"), lambda: so1.at[j, pl.ds(0, 3 * own_block), wide])
+            last = ((t, "last"), lambda: so1.at[p, j, pl.ds(0, 3 * own_block), wide])
             send((t, "far"), "x2", [(t, "add")], at(2), slot(0), slot(0), size, prio, sent_x, last)
             send((t, "plus"), "x+", [(t, "add")], at(1), slot(1), slot(1), size, prio, sent_x, last)
             send((t, "minus"), "x-", [(t, "add")], at(-1), slot(2), slot(2), size, prio, sent_x, last)
             terms, from_others = (0, 1, 2), [(t, "far"), (t, "plus"), (t, "minus")]
         else:
-            last = ((t, "last"), lambda: so1.at[j, pl.ds(0, 2 * own_block), wide])
+            last = ((t, "last"), lambda: so1.at[p, j, pl.ds(0, 2 * own_block), wide])
             send((t, "relay"), "x" + d, [(t, "add")], at(2), slot(0), slot(0), size, prio, sent_x)
             send((t, "direct"), "x" + e, [(t, "add")], at(-s), slot(2), slot(2), size, prio + 0.5, sent_x, last)
 
             def add_relay():
-                so1[j, in_half(s), wide] = (
-                    so1[j, in_half(s), wide].astype(f32) + in1[j, 0, :, wide].astype(f32)).astype(bf16)
+                so1[p, j, in_half(s), wide] = (
+                    so1[p, j, in_half(s), wide].astype(f32) + in1[p, j, 0, :, wide].astype(f32)).astype(bf16)
 
             compute((t, "radd"), [(t, "relay")], add_relay, prio, 0.05)
             send((t, "final"), "x" + d, [(t, "radd")], at(s), slot(1), slot(1), size, prio, sent_x, last)
             terms, from_others = (1, 2), [(t, "final"), (t, "direct")]
 
         def finish():
-            total = so1[j, in_half(0), wide].astype(f32)
+            total = so1[p, j, in_half(0), wide].astype(f32)
             for i in terms:
-                total = total + in1[j, i, :, wide].astype(f32)
-            cs1[j, late_rows(), wide] = total.astype(bf16)
+                total = total + in1[p, j, i, :, wide].astype(f32)
+            cs1[p, j, late_rows(), wide] = total.astype(bf16)
 
         compute((t, "finish"), from_others, finish, prio, 0.06)
 
         def there(*where, **more):
-            return lambda: cs1.at[j, late_rows(*where, **more), wide]
+            return lambda: cs1.at[p, j, late_rows(*where, **more), wide]
 
         begin = [(t, "finish")]
-        paired = ((t, "P"), lambda: cs1.at[j, pl.ds(0, half_of), wide])
+        paired = ((t, "P"), lambda: cs1.at[p, j, pl.ds(0, half_of), wide])
         other = 1 - c
         send((t, "A", "+"), "x+", begin, there(0), there(0), there(-1), size, prio, sent_x)
         send((t, "A", "-"), "x-", begin, there(0), there(0), there(1), size, prio, sent_x)
@@ -506,46 +513,59 @@
 
         def count():
             def step(i, _):
-                rows = pl.ds(pl.multiple_of(i * 64, 64), 64)
+                here = pl.ds(pl.multiple_of(i * 64, 64), 64)
+                rows = pl.ds(pl.multiple_of(p * PART + i * 64, 64), 64)
+                shift, one, two = stats[0, rows, :], stats[1, rows, :], stats[2, rows, :]
                 for at, cols in enumerate(columns):
                     value = (residual_scale * first[rows, cols].astype(f32)
-                             + cs1[j, rows, at * GROUP:(at + 1) * GROUP].astype(f32))
+                             + cs1[p, j, here, at * GROUP:(at + 1) * GROUP].astype(f32))
                     val[rows, cols] = value
-                    if j == 0 and at == 0:
-                        stats[0, rows, :] = jnp.mean(value, -1, keepdims=True)
-                    value = value - stats[0, rows, :]
-                    one = jnp.sum(value, -1, keepdims=True)
-                    two = jnp.sum(value * value, -1, keepdims=True)
-                    if j == 0 and at == 0:
-                        stats[1, rows, :], stats[2, rows, :] = one, two
-                    else:
-                        stats[1, rows, :] += one
-                        stats[2, rows, :] += two
+                    for lanes in range(0, GROUP, 128):
+                        part = value[:, lanes:lanes + 128] - shift
+                        one, two = one + part, two + part * part
+                stats[1, rows, :], stats[2, rows, :] = one, two
                 return 0
 
-            lax.fori_loop(0, SEQ // 64, step, 0)
-
-        compute((t, "count"), begin + far + [(t, "P", dx) for dx in (0, -1, 1, 2)]
-                + ([("late", j - 1, "count")] if j else []), count, prio, 0.3 * len(dists))
-        ops[-1].name = ("late", j, "count")
-
-    for j, dists in enumerate(LATE):
-        late_chunk(j, dists, DIRECT[j], 2 + 0.1 * j)
-
-    def finish_norm():
+            lax.fori_loop(0, PART // 64, step, 0)
+
+        compute((t, "count"), begin + far + [("stats", p)] + [(t, "P", dx) for dx in (0, -1, 1, 2)],
+                count, prio + 1, 0.15 * len(dists))
+
+    def begin_stats(p):
+        def emit():
+            rows = pl.ds(p * PART, PART)
+            shift = residual_scale * first[rows, 0:128].astype(f32)[:, 0:1]
+            stats[0, rows, :] = jnp.broadcast_to(shift, (PART, 128))
+            stats[1, rows, :] = jnp.zeros((PART, 128), f32)
+            stats[2, rows, :] = jnp.zeros((PART, 128), f32)
+
+        compute(("stats", p), [("hidden", p, 1)], emit, 6, 0.1)
+
+    for p in range(PARTS):
+        begin_stats(p)
+        for j, dists in enumerate(LATE):
+            late_chunk(p, j, dists, DIRECT[j], 2 + 0.5 * p + 0.05 * j)
+
+    def finish_norm(p):
         def step(i, _):
-            rows = pl.ds(pl.multiple_of(i * 64, 64), 64)
-            off = stats[1, rows, :] * (1.0 / WIDTH)
-            variance = jnp.maximum(stats[2, rows, :] * (1.0 / WIDTH) - off * off, 0.0)
-            scale = lax.rsqrt(variance + norm_epsilon)
-            centered = val[rows, :] - (stats[0, rows, :] + off)
+            rows = pl.ds(pl.multiple_of(p * PART + i * 64, 64), 64)
+            off = jnp.sum(stats[1, rows, :], -1, keepdims=True) * (1.0 / WIDTH)
+            square = jnp.sum(stats[2, rows, :], -1, keepdims=True) * (1.0 / WIDTH)
+            scale = lax.rsqrt(jnp.maximum(square - off * off, 0.0) + norm_epsilon)
+            centered = val[rows, :] - (stats[0, rows, 0:1] + off)
             res[rows, :] = (centered * scale * cgain[...] + cshift[...]).astype(bf16)
             return 0
 
-        lax.fori_loop(0, SEQ // 64, step, 0)
-
-    compute("finish_norm", [("late", j, "count") for j in range(len(LATE))], finish_norm, 0, 1.2)
-
+        lax.fori_loop(0, PART // 64, step, 0)
+
+    for p in range(PARTS):
+        compute(("finish_norm", p), [(("late", p, j), "count") for j in range(len(LATE))],
+                functools.partial(finish_norm, p), 6, 0.65)
+
+    for tag, way, _, _ in PIECES:
+        for op in ops:
+            if isinstance(op.name, tuple) and op.name[0] == tag:
+                op.earliest = EARLIEST.get(tag[0] + way, 0.0)
     order, done = plan(ops)
     if report is not None:
         report(order, done, len(send_groups), len(recv_groups), len(loads))
@@ -579,7 +599,7 @@
         wait()
 
 
-N_SENDS, N_RECVS, N_LOADS = 37, 205, 7
+N_SENDS, N_RECVS, N_LOADS = 50, 261, 7
 
 
 def local(tokens, gate_outer, gate_inner, conv_input, mixer_output, conv_taps, mixer_gain,
@@ -608,13 +628,13 @@
             pltpu.VMEM((PARTS, OWN, WIDTH), f32),
             pltpu.VMEM((SEQ, WIDTH), bf16),
             pltpu.VMEM((SEQ, 1024), bf16),
-            pltpu.VMEM((len(LATE), SEQ, CHUNK), bf16),
-            pltpu.VMEM((len(LATE), SEQ // 2, CHUNK), bf16),
-            pltpu.VMEM((len(LATE), SEQ // 2, CHUNK), bf16),
-            pltpu.VMEM((len(LATE), 3, ROWS, CHUNK), bf16),
-            pltpu.VMEM((len(LATE), SEQ, CHUNK), bf16),
+            pltpu.VMEM((PARTS, len(LATE), PART, CHUNK), bf16),
+            pltpu.VMEM((PARTS, len(LATE), CORE_ROWS, CHUNK), bf16),
+            pltpu.VMEM((PARTS, len(LATE), CORE_ROWS, CHUNK), bf16),
+            pltpu.VMEM((PARTS, len(LATE), 3, OWN, CHUNK), bf16),
+            pltpu.VMEM((PARTS, len(LATE), PART, CHUNK), bf16),
             pltpu.VMEM((SEQ, WIDTH), f32),
-            pltpu.VMEM((3, SEQ, 1), f32),
+            pltpu.VMEM((3, SEQ, 128), f32),
             pltpu.SemaphoreType.DMA((N_SENDS,)),
             pltpu.SemaphoreType.DMA((N_RECVS,)),
             pltpu.SemaphoreType.DMA((N_LOADS,)),

time: 109 us -> 102 us (0.936)
  Pallas kernels: 108 us -> 101 us
    pallas_call x1, Pallas kernels: 108 us -> 101 us  [local(): pl.pallas_call(layer_kernel, out_shape=pltpu.VMEM((SEQ, WIDTH), bf16), in...]
where the time goes in v6:
time: 102 us
  Pallas kernels  101 us (99%)
  local copies, waits for them, and re-layouts  1.32 us (1%)
    pallas_call x1, Pallas kernels, local(): pl.pallas_call(layer_kernel, out_shape=pltpu.VMEM((SEQ, WIDTH), bf16), in...  101 us

profile of v6, /device:TPU:1, one launch (start us, length us, event | category | flops | bytes accessed | tf_op | source)
XLA Modules:
  0.0 102.0 jit_solution(13684917623742930432)
XLA Ops:
  0.0 100.6 %shard_map.118 = bf16[512,2048]{1,0:T(8,128)(2,1)S(1)} custom-call(bf16[512,2048]{1,0:T(8,128)(2,1)} %tok_hbm.1, bf16[64,128]{1,0:T(8,128)(2,1)} %go_hbm.1, bf16[64,128]{1,0:T(8,128)(2,1)} %gi_hbm.1, bf16[64,128]{1,0:T(8,128)(2,1)} %ci_hbm.1, bf16[64,128]{1,0:T(8,128)(2,1)} %mo_hbm.1, bf16[64,1024]{1,0:T(8,128)(2,1)} %up_hbm.1, bf16[64,1024]{1,0:T(8,128)(2,1)} %dn_hbm.1, ...), custom_call_target="tpu_custom_call" | custom-call | tf_op jit(solution)/shard_map/pallas_call | solution.py:609
  100.6 1.3 %copy.14 = bf16[512,2048]{1,0:T(8,128)(2,1)} copy(bf16[512,2048]{1,0:T(8,128)(2,1)S(1)} %shard_map.118) | data formatting | bytes 4194304

commit v7 on v6

--- a/solution.py
+++ b/solution.py
@@ -21,12 +21,12 @@
 NEAR = ("+", "-")
 ARRIVAL = (0, 1, -1, 2, -2, 3, -3, 4)
 LATE = ((0, 1), (-1, 2), (-2, 3), (-3,), (4,))
-DIRECT = (False, False, False, True, True)
-
-LINK_RATE, LINK_LAT = 46.6e3, 1.9
-PAIR_RATE, PAIR_LAT = 500e3, 1.1
-BACKLOG = 2.39
-PATHS = {"c": (PAIR_RATE, PAIR_LAT), "x2": (LINK_RATE, 2.6)}
+DIRECT = (False, False, False, False, True)
+
+LINK_RATE, LINK_LAT = 45.0e3, 2.1
+PAIR_RATE, PAIR_LAT = 400e3, 1.6
+BACKLOG = 2.19
+PATHS = {"c": (PAIR_RATE, PAIR_LAT), "x+": (LINK_RATE, 2.6), "x-": (LINK_RATE, 2.6)}
 
 
 PIECES = (
@@ -41,14 +41,14 @@
     ("d2", "z", 512, 5),
 )
 HOPS = {
-    "m": {"y": (2.13, 0.62), "yz": (5.5, 0.56, 5.79, 3.68),
-          "z": (1.2, 3.12, 3.32, 4.69), "zy": (4.31, 4.14, 4.44, 5.8, 5.47)},
-    "u": {"y": (4.44, 2.55), "yz": (6, 3.2, 6, 1.93),
-          "z": (0.3, 5.81, 6, 3.59), "zy": (0.72, 0.66, 0.77, 6, 1.06)},
-    "d": {"y": (4.84, 3.77), "yz": (2.16, 3.17, 1.76, 5.74),
-          "z": (0.3, 3.82, 4.28, 6), "zy": (3.88, 1.07, 5.66, 2.05, 2.8)},
+    "m": {"y": (5.61, 4.34), "yz": (5.34, 6, 0.53, 6),
+          "z": (4.44, 4.62, 0.82, 4.99), "zy": (5.9, 4.34, 4.14, 4.25, 4.06)},
+    "u": {"y": (2.22, 1.12), "yz": (3.71, 6, 1.21, 5.27),
+          "z": (0.3, 3.75, 0.94, 1.15), "zy": (6, 0.54, 3.36, 1.2, 3.15)},
+    "d": {"y": (5.58, 3.55), "yz": (0.71, 1.27, 1.04, 6),
+          "z": (0.3, 0.72, 2.95, 5.59), "zy": (4.92, 2.2, 2.34, 2.56, 1.36)},
 }
-EARLIEST = {"uz": 7.5, "dy": 8.8, "dz": 15.2}
+EARLIEST = {"uy": 6.0, "uz": 11.0, "dy": 16.3, "dz": 19.5}
 
 
 class Op:
@@ -75,7 +75,7 @@
                 continue
             ready = max([done[d] for d in op.deps] + [op.earliest])
             if op.link is not None:
-                ready = max(ready, link_free.get(op.link, 0.0) - (BACKLOG if op.prio >= 3 else 0.65 * BACKLOG))
+                ready = max(ready, link_free.get(op.link, 0.0) - (BACKLOG if op.prio >= 3 else 0.73 * BACKLOG))
             key = (max(ready, now), op.prio, at)
             if best is None or key < best[0]:
                 best = (key, op)
@@ -141,7 +141,8 @@
         all_here = group[1] if group else landed
         sends.setdefault(sent[0], lambda: copy(sent[1](), sent[1]()).wait_send())
         op = Op(
-            name, deps, lambda: copy(src(), dst()).start(), prio, link=link, nbytes=nbytes,
+            name, deps, lambda: copy(src(), dst()).start(), prio,
+            link="x+" if link == "x2" else link, nbytes=2 * nbytes if link == "x2" else nbytes,
             wait=lambda: copy(all_here(), all_here()).wait_recv(),
         )
         op.group = group[0] if group else None
@@ -560,7 +561,7 @@
 
     for p in range(PARTS):
         compute(("finish_norm", p), [(("late", p, j), "count") for j in range(len(LATE))],
-                functools.partial(finish_norm, p), 6, 0.65)
+                functools.partial(finish_norm, p), 6, 1.05)
 
     for tag, way, _, _ in PIECES:
         for op in ops:
@@ -599,7 +600,7 @@
         wait()
 
 
-N_SENDS, N_RECVS, N_LOADS = 50, 261, 7
+N_SENDS, N_RECVS, N_LOADS = 50, 263, 7
 
 
 def local(tokens, gate_outer, gate_inner, conv_input, mixer_output, conv_taps, mixer_gain,

time: 102 us -> 103 us (level)
  no operation moved by 1% of the time
where the time goes in v7:
time: 103 us
  Pallas kernels  101 us (98%)
  local copies, waits for them, and re-layouts  1.32 us (1%)
    pallas_call x1, Pallas kernels, local(): pl.pallas_call(layer_kernel, out_shape=pltpu.VMEM((SEQ, WIDTH), bf16), in...  101 us

profile of v7, /device:TPU:1, one launch (start us, length us, event | category | flops | bytes accessed | tf_op | source)
XLA Modules:
  0.0 102.7 jit_solution(5317189042518632963)
XLA Ops:
  0.0 101.4 %shard_map.118 = bf16[512,2048]{1,0:T(8,128)(2,1)S(1)} custom-call(bf16[512,2048]{1,0:T(8,128)(2,1)} %tok_hbm.1, bf16[64,128]{1,0:T(8,128)(2,1)} %go_hbm.1, bf16[64,128]{1,0:T(8,128)(2,1)} %gi_hbm.1, bf16[64,128]{1,0:T(8,128)(2,1)} %ci_hbm.1, bf16[64,128]{1,0:T(8,128)(2,1)} %mo_hbm.1, bf16[64,1024]{1,0:T(8,128)(2,1)} %up_hbm.1, bf16[64,1024]{1,0:T(8,128)(2,1)} %dn_hbm.1, ...), custom_call_target="tpu_custom_call" | custom-call | tf_op jit(solution)/shard_map/pallas_call | solution.py:610
  101.4 1.3 %copy.14 = bf16[512,2048]{1,0:T(8,128)(2,1)} copy(bf16[512,2048]{1,0:T(8,128)(2,1)S(1)} %shard_map.118) | data formatting | bytes 4194304

commit v8 on v7

--- a/solution.py
+++ b/solution.py
@@ -20,12 +20,12 @@
 CHUNKS, CHUNK = 4, 512
 NEAR = ("+", "-")
 ARRIVAL = (0, 1, -1, 2, -2, 3, -3, 4)
-LATE = ((0, 1), (-1, 2), (-2, 3), (-3,), (4,))
-DIRECT = (False, False, False, False, True)
+LATE = ((0, 1), (-1, 2), (-2, 3), (-3, 4))
+DIRECT = (False, False, False, False)
 
 LINK_RATE, LINK_LAT = 45.0e3, 2.1
 PAIR_RATE, PAIR_LAT = 400e3, 1.6
-BACKLOG = 2.19
+BACKLOG = 1.9
 PATHS = {"c": (PAIR_RATE, PAIR_LAT), "x+": (LINK_RATE, 2.6), "x-": (LINK_RATE, 2.6)}
 
 
@@ -41,14 +41,14 @@
     ("d2", "z", 512, 5),
 )
 HOPS = {
-    "m": {"y": (5.61, 4.34), "yz": (5.34, 6, 0.53, 6),
-          "z": (4.44, 4.62, 0.82, 4.99), "zy": (5.9, 4.34, 4.14, 4.25, 4.06)},
-    "u": {"y": (2.22, 1.12), "yz": (3.71, 6, 1.21, 5.27),
-          "z": (0.3, 3.75, 0.94, 1.15), "zy": (6, 0.54, 3.36, 1.2, 3.15)},
-    "d": {"y": (5.58, 3.55), "yz": (0.71, 1.27, 1.04, 6),
-          "z": (0.3, 0.72, 2.95, 5.59), "zy": (4.92, 2.2, 2.34, 2.56, 1.36)},
+    "m": {"y": (0.76, 3.57), "yz": (5.4, 4.91, 3.59, 6),
+          "z": (0.75, 4.7, 5.55, 2.49), "zy": (6, 4.33, 6, 3.75, 3.57)},
+    "u": {"y": (3.62, 4.53), "yz": (3.69, 1.44, 4.5, 2.13),
+          "z": (1.42, 1.1, 0.76, 3.22), "zy": (0.3, 0.99, 3.35, 3.91, 1.5)},
+    "d": {"y": (5.22, 3.72), "yz": (6, 1.71, 5.65, 1.31),
+          "z": (1.86, 2.09, 0.83, 2.25), "zy": (2.19, 0.3, 1.5, 2.04, 2.99)},
 }
-EARLIEST = {"uy": 6.0, "uz": 11.0, "dy": 16.3, "dz": 19.5}
+EARLIEST = {"uy": 3.8, "uz": 11.0, "dy": 15.3, "dz": 0.1}
 
 
 class Op:
@@ -75,7 +75,7 @@
                 continue
             ready = max([done[d] for d in op.deps] + [op.earliest])
             if op.link is not None:
-                ready = max(ready, link_free.get(op.link, 0.0) - (BACKLOG if op.prio >= 3 else 0.73 * BACKLOG))
+                ready = max(ready, link_free.get(op.link, 0.0) - (BACKLOG if op.prio >= 3 else 0.94 * BACKLOG))
             key = (max(ready, now), op.prio, at)
             if best is None or key < best[0]:
                 best = (key, op)
@@ -600,7 +600,7 @@
         wait()
 
 
-N_SENDS, N_RECVS, N_LOADS = 50, 263, 7
+N_SENDS, N_RECVS, N_LOADS = 46, 250, 7
 
 
 def local(tokens, gate_outer, gate_inner, conv_input, mixer_output, conv_taps, mixer_gain,

time: 103 us -> 98.7 us (0.958)
  Pallas kernels: 101 us -> 97.2 us
    pallas_call x1, Pallas kernels: 101 us -> 97.2 us  [local(): pl.pallas_call(layer_kernel, out_shape=pltpu.VMEM((SEQ, WIDTH), bf16), in...]
where the time goes in v8:
time: 98.7 us; the launch traced here: 98.5 us
  Pallas kernels  97.2 us (98%)
  local copies, waits for them, and re-layouts  1.32 us (1%)
    pallas_call x1, Pallas kernels, local(): pl.pallas_call(layer_kernel, out_shape=pltpu.VMEM((SEQ, WIDTH), bf16), in...  97.2 us

profile of v8, /device:TPU:1, one launch (start us, length us, event | category | flops | bytes accessed | tf_op | source)
XLA Modules:
  0.0 98.5 jit_solution(9595282486748209896)
XLA Ops:
  0.0 97.2 %shard_map.118 = bf16[512,2048]{1,0:T(8,128)(2,1)S(1)} custom-call(bf16[512,2048]{1,0:T(8,128)(2,1)} %tok_hbm.1, bf16[64,128]{1,0:T(8,128)(2,1)} %go_hbm.1, bf16[64,128]{1,0:T(8,128)(2,1)} %gi_hbm.1, bf16[64,128]{1,0:T(8,128)(2,1)} %ci_hbm.1, bf16[64,128]{1,0:T(8,128)(2,1)} %mo_hbm.1, bf16[64,1024]{1,0:T(8,128)(2,1)} %up_hbm.1, bf16[64,1024]{1,0:T(8,128)(2,1)} %dn_hbm.1, ...), custom_call_target="tpu_custom_call" | custom-call | tf_op jit(solution)/shard_map/pallas_call | solution.py:610
  97.2 1.3 %copy.14 = bf16[512,2048]{1,0:T(8,128)(2,1)} copy(bf16[512,2048]{1,0:T(8,128)(2,1)S(1)} %shard_map.118) | data formatting | bytes 4194304

commit v9 on v8

--- a/solution.py
+++ b/solution.py
@@ -119,8 +119,10 @@
 
     peer = {
         "z+": device(dz=1), "z-": device(dz=-1), "y+": device(dy=1), "y-": device(dy=-1),
-        "x+": device(dx=1), "x-": device(dx=-1), "x2": device(dx=2), "c": device(dc=1),
+        "x+": device(dx=1), "x-": device(dx=-1), "c": device(dc=1),
     }
+    if any(DIRECT):
+        peer["x2"] = device(dx=2)
     sign = {"+": 1, "-": -1}
 
     ops = []

time: 98.7 us -> 98.5 us (level)
  no operation moved by 1% of the time
where the time goes in v9:
time: 98.5 us; the launch traced here: 98.2 us
  Pallas kernels  96.9 us (98%)
  local copies, waits for them, and re-layouts  1.32 us (1%)
    pallas_call x1, Pallas kernels, local(): pl.pallas_call(layer_kernel, out_shape=pltpu.VMEM((SEQ, WIDTH), bf16), in...  96.9 us

profile of v9, /device:TPU:1, one launch (start us, length us, event | category | flops | bytes accessed | tf_op | source)
XLA Modules:
  0.0 98.2 jit_solution(7014629286953157688)
XLA Ops:
  0.0 96.9 %shard_map.118 = bf16[512,2048]{1,0:T(8,128)(2,1)S(1)} custom-call(bf16[512,2048]{1,0:T(8,128)(2,1)} %tok_hbm.1, bf16[64,128]{1,0:T(8,128)(2,1)} %go_hbm.1, bf16[64,128]{1,0:T(8,128)(2,1)} %gi_hbm.1, bf16[64,128]{1,0:T(8,128)(2,1)} %ci_hbm.1, bf16[64,128]{1,0:T(8,128)(2,1)} %mo_hbm.1, bf16[64,1024]{1,0:T(8,128)(2,1)} %up_hbm.1, bf16[64,1024]{1,0:T(8,128)(2,1)} %dn_hbm.1, ...), custom_call_target="tpu_custom_call" | custom-call | tf_op jit(solution)/shard_map/pallas_call | solution.py:612
  96.9 1.3 %copy.14 = bf16[512,2048]{1,0:T(8,128)(2,1)} copy(bf16[512,2048]{1,0:T(8,128)(2,1)S(1)} %shard_map.118) | data formatting | bytes 4194304
